TPU v7x, 32 devices: a whole 2x2x4 slice. The times are simulated.
32 devices in a mesh: sp: 8 (over z, y), tp: 4 (over x, core).
Axes of the slice: x: 2, y: 2, z: 4, core: 2. Of those that a mesh axis runs over, the one named last changes fastest.
Arguments:
- queries: bfloat16 [6144, 1024], P('sp', 'tp'), may hold values from -6 to 6
- keys: bfloat16 [6144, 1024], P('sp', 'tp'), may hold values from -6 to 6
- values: bfloat16 [6144, 2048], P('sp', 'tp'), may hold values from -6 to 6
- out_gate: bfloat16 [6144, 2048], P('sp', 'tp'), may hold values from -6 to 6
- input_gates: float32 [2, 4, 6144], P(None, 'tp', 'sp'), may hold values from -4 to 300
- forget_gates: float32 [2, 4, 6144], P(None, 'tp', 'sp'), may hold values from -1 to 16
- doc_ids: int32 [6144], P('sp'), may hold values from 0 to 3, never falling along the last dimension, each value on 1 to 3072 neighbouring positions
- head_gain: float32 [2048], P('tp'), may hold values from 0.1 to 1.9
- w_out: bfloat16 [2048, 2048], P('tp'), may hold values from -0.25 to 0.25
- resid: bfloat16 [6144, 2048], P(('sp', 'tp')), may hold values from -30 to 30
- norm_gain: float32 [2048], replicated, may hold values from 0.1 to 1.9
- w_up: bfloat16 [2048, 8192], P('sp', 'tp'), may hold values from -0.125 to 0.125
- w_down: bfloat16 [8192, 2048], P('tp', 'sp'), may hold values from -0.0625 to 0.0625
Outputs:
- layer_out: bfloat16 [6144, 2048], P(('sp', 'tp'))
Inputs may be any that keep to these rules, and one draw needn't show every extreme that they name: `doc_ids`: document numbers never fall along the positions.
All inputs are finite; a program needn't handle non-finite values.
Results may differ from a plain program's by a relative error of at most 0.013.
Values may be sent and summed in bfloat16 or wider, within the bound.
No kernel may reach another device: no remote copies, remote signals or barrier semaphores. Data moves between devices by JAX's collectives and lax.ppermute only.
A program may use at most 128 MiB of HBM per device.

v0:
```python
import functools

import jax
import jax.numpy as jnp
from jax import lax
from jax.experimental import pallas as pl
from jax.experimental.pallas import tpu as pltpu
from jax.sharding import PartitionSpec as P

EPS = 1e-06
FAR_LOW = -1e30
LONGEST_DOC = 3072
EXTRA = 128


def places(axis):
    outer = lax.axis_size(axis) // 2
    assert outer * 2 == lax.axis_size(axis)
    index = lax.axis_index(axis)
    return outer, index // 2, index % 2


def flip(value, axis):
    return lax.ppermute(value, axis, [(i, i ^ 1) for i in range(lax.axis_size(axis))])


def shift(value, axis, step, cross=0):
    outer = lax.axis_size(axis) // 2
    moves = [
        (2 * a + c, 2 * ((a + step) % outer) + (c ^ cross)) for a in range(outer) for c in range(2)
    ]
    return lax.ppermute(value, axis, moves)


def carry_shift(value, step):
    outer = lax.axis_size("sp") // 2
    moves = [(2 * a, 2 * (a - step)) for a in range(step, outer)]
    moves += [(2 * a + 1, 2 * (a + step) + 1) for a in range(outer - step)]
    return lax.ppermute(value, "sp", moves)


def running_sums(rows):
    length = rows.shape[1]
    lane = lax.broadcasted_iota(jnp.int32, rows.shape, 1)
    left, right = rows, rows
    step = 1
    while step < length:
        left = left + jnp.where(lane >= step, pltpu.roll(left, step, 1), 0.0)
        right = right + jnp.where(lane < length - step, pltpu.roll(right, length - step, 1), 0.0)
        step *= 2
    return left, right


def log_sigmoid(x):
    return jnp.minimum(x, 0.0) - jnp.log1p(jnp.exp(-jnp.abs(x)))


def three_parts(x):
    high = x.astype(jnp.bfloat16).astype(jnp.float32)
    rest = x - high
    mid = rest.astype(jnp.bfloat16).astype(jnp.float32)
    return high, mid, rest - mid


def pack_side(sums, peak, total, edge, shape):
    lane = lax.broadcasted_iota(jnp.int32, shape, 1)
    high = sums.astype(jnp.bfloat16).astype(jnp.float32)
    side = jnp.where(lane == 0, high, jnp.where(lane == 1, sums - high, 0.0))
    for at, part in enumerate(three_parts(peak) + three_parts(total) + (edge,)):
        side = jnp.where(lane == 2 + at, part, side)
    return side.astype(jnp.bfloat16)


def merge(states, valid, dv):
    between = jnp.zeros((1, 1), jnp.float32)
    heights, links = [], []
    for state, there in zip(states, valid):
        side = state[:16, dv:].astype(jnp.float32)[:1]
        peak = side[:, 2:3] + side[:, 3:4] + side[:, 4:5]
        total = side[:, 5:6] + side[:, 6:7] + side[:, 7:8]
        edge = side[:, 8:9]
        wanted = wanted if links else edge
        link = jnp.logical_and(edge == wanted, edge >= 0.0)
        if there is not None:
            link = jnp.logical_and(link, there)
        heights.append(jnp.where(link, peak + between, FAR_LOW))
        links.append(link)
        between = between + total
    top = heights[0]
    for height in heights[1:]:
        top = jnp.maximum(top, height)
    carry = None
    for state, height, link in zip(states, heights, links):
        part = jnp.where(link, jnp.exp(height - top), 0.0) * state[...].astype(jnp.float32)
        carry = part if carry is None else carry + part
    return carry, top, between, jnp.where(links[0], wanted, -1.0)


def put_state(out, carry, top, total, edge, dv):
    out[:, :dv] = carry[:, :dv].astype(jnp.bfloat16)
    sums = carry[:, dv : dv + 1] + carry[:, dv + 1 : dv + 2]
    out[:, dv:] = pack_side(sums, top, total, edge, (carry.shape[0], EXTRA))


def summary_kernel(info, keys, values, gates, give, mine):
    dqk = keys.shape[1]
    dv = values.shape[1]
    length = keys.shape[0]
    rows = gates[...]
    left, right = running_sums(log_sigmoid(rows))
    doc = rows[4:5]
    first, last = doc[:, :1], doc[:, length - 1 :]
    keys_t = keys[...].astype(jnp.float32).T
    vals = values[...]
    upper = info[0] == 1
    for cum, total, in_gate, edge, holder in (
        (left[2:3], left[2:3, length - 1 :], rows[0:1], last, upper),
        (right[3:4], right[3:4, :1], rows[1:2], first, jnp.logical_not(upper)),
    ):
        exponent = jnp.where(doc == edge, total - cum + in_gate, FAR_LOW)
        peak = jnp.max(exponent, axis=1, keepdims=True)
        weighted = (keys_t * jnp.exp(exponent - peak)).astype(jnp.bfloat16)
        memory = jnp.dot(weighted, vals, preferred_element_type=jnp.float32).astype(jnp.bfloat16)
        sums = jnp.sum(weighted.astype(jnp.float32), axis=1, keepdims=True)
        side = pack_side(sums, peak, total, edge, (dqk, EXTRA))

        @pl.when(holder)
        def _():
            mine[:, :dv] = memory
            mine[:, dv:] = side

        @pl.when(jnp.logical_not(holder))
        def _():
            give[:, :dv] = memory
            give[:, dv:] = side


SMALL = pl.BlockSpec(memory_space=pltpu.SMEM)
LOCAL = pl.BlockSpec(memory_space=pltpu.VMEM)


def summaries(info, keys, values, gates):
    shape = jax.ShapeDtypeStruct((keys.shape[1], values.shape[1] + EXTRA), jnp.bfloat16)
    return pl.pallas_call(
        summary_kernel,
        out_shape=(shape, shape),
        in_specs=[SMALL, LOCAL, LOCAL, LOCAL],
        name="summary",
    )(info, keys, values, gates)


def pair_kernel(mine, got, out):
    dv = mine.shape[1] - EXTRA
    put_state(out, *merge((mine, got), (None, None), dv), dv)


def pair_state(mine, got):
    return pl.pallas_call(
        pair_kernel, out_shape=jax.ShapeDtypeStruct(mine.shape, mine.dtype), name="pair"
    )(mine, got)


def lead_kernel(info, *refs):
    states, out = refs[:-1], refs[-1]
    dv = out.shape[1] - EXTRA
    valid = [info[1] > j for j in range(len(states))]
    put_state(out, *merge(states, valid, dv), dv)


def lead_state(info, states):
    return pl.pallas_call(
        lead_kernel,
        out_shape=jax.ShapeDtypeStruct(states[0].shape, states[0].dtype),
        in_specs=[SMALL] + [LOCAL] * len(states),
        name="lead",
    )(info, *states)


def emit_kernel(reach, info, queries, keys, values, gates, out_gate, gain, *rest):
    states, handed = rest[: reach + 1], rest[reach + 1]
    readout, row_buf, col_buf, carry_hi, carry_lo, top_buf = rest[reach + 2 :]
    _, dv = values.shape
    tile = queries.shape[0]
    step = pl.program_id(0)
    scale = queries.shape[1] ** (-0.5)

    @pl.when(step == 0)
    def _():
        rows = gates[...]
        left, right = running_sums(log_sigmoid(rows))
        doc = rows[4:5]
        cums = [left[2:3], right[3:4], rows[0:1] - left[2:3], rows[1:2] - right[3:4]]
        pack = jnp.concatenate(cums + [doc] * 4, axis=0)
        row_buf[...] = pack
        col_buf[...] = pack.T
        valid = [None] + [info[1] > j for j in range(reach)]
        held = 1 - info[0]
        for way, got, there in ((held, states, valid), (info[0], (handed,), (None,))):
            carry, top, _, edge = merge(got, there, dv)
            high = carry.astype(jnp.bfloat16)
            carry_hi[way] = high
            carry_lo[way] = (carry - high.astype(jnp.float32)).astype(jnp.bfloat16)
            top_buf[way] = jnp.broadcast_to(jnp.concatenate([top, edge], axis=0), (2, 128))

    query = queries[...]
    scores = (
        lax.dot_general(
            query, keys[...], (((1,), (1,)), ((), ())), preferred_element_type=jnp.float32
        )
        * scale
    )
    cols = col_buf[pl.ds(step * tile, tile), :]
    rows = row_buf[...]
    at_t = step * tile + lax.broadcasted_iota(jnp.int32, scores.shape, 0)
    at_s = lax.broadcasted_iota(jnp.int32, scores.shape, 1)
    same = cols[:, 4:5] == rows[4:5]
    mixed = None
    memory = None
    for way in range(2):
        order = at_t >= at_s if way == 0 else at_t <= at_s
        keep = jnp.logical_and(order, same)
        cum = cols[:, way : way + 1]
        inside = rows[2 + way : 3 + way]
        usable = cols[:, 4:5] == top_buf[way, 1:2, :1]
        carried = jnp.where(usable, cum + top_buf[way, :1, :1], FAR_LOW)
        peak = jnp.maximum(
            carried, cum + jnp.max(jnp.where(keep, inside, FAR_LOW), axis=1, keepdims=True)
        )
        weights = jnp.where(keep, scores * jnp.exp(inside + (cum - peak)), 0.0)
        inter = jnp.where(usable, jnp.exp(carried - peak), 0.0) * scale
        got = jnp.dot(query, carry_hi[way], preferred_element_type=jnp.float32) + jnp.dot(
            query, carry_lo[way], preferred_element_type=jnp.float32
        )
        denom = jnp.sum(weights, axis=1, keepdims=True) + inter * (
            got[:, dv : dv + 1] + got[:, dv + 1 : dv + 2]
        )
        share = 1.0 / jnp.maximum(jnp.abs(denom), 1.0)
        part = weights * share
        mixed = part if mixed is None else mixed + part
        part = got[:, :dv] * (inter * share)
        memory = part if memory is None else memory + part
    memory = memory + jnp.dot(
        mixed.astype(jnp.bfloat16), values[...], preferred_element_type=jnp.float32
    )
    factor = lax.rsqrt(jnp.mean(memory * memory, axis=1, keepdims=True) + EPS)
    gate = 1.0 / (1.0 + jnp.exp(-out_gate[...].astype(jnp.float32)))
    readout[...] = (memory * factor * gain[...] * gate).astype(jnp.bfloat16)


def emit(info, queries, keys, values, gates, out_gate, gain, states, handed):
    length, dqk = queries.shape
    dv = values.shape[1]
    tile = length // 3 if length % 384 == 0 else length
    whole = lambda a: pl.BlockSpec(a.shape, lambda i, *_: (0,) * a.ndim)
    by_rows = lambda width: pl.BlockSpec((tile, width), lambda i, *_: (i, 0))
    return pl.pallas_call(
        functools.partial(emit_kernel, len(states) - 1),
        out_shape=jax.ShapeDtypeStruct((length, dv), jnp.bfloat16),
        grid_spec=pltpu.PrefetchScalarGridSpec(
            num_scalar_prefetch=1,
            grid=(length // tile,),
            in_specs=[
                by_rows(dqk),
                whole(keys),
                whole(values),
                whole(gates),
                by_rows(dv),
                whole(gain),
            ]
            + [whole(s) for s in (*states, handed)],
            out_specs=by_rows(dv),
            scratch_shapes=[
                pltpu.VMEM((8, length), jnp.float32),
                pltpu.VMEM((length, 8), jnp.float32),
                pltpu.VMEM((2, dqk, dv + EXTRA), jnp.bfloat16),
                pltpu.VMEM((2, dqk, dv + EXTRA), jnp.bfloat16),
                pltpu.VMEM((2, 2, 128), jnp.float32),
            ],
        ),
        name="emit",
    )(info, queries, keys, values, gates, out_gate, gain, *states, handed)


def project_kernel(count, *refs):
    pieces, weights = refs[:count], refs[count : 2 * count]
    resid, gain, mixed_out, normed_out = refs[2 * count :]
    mixed = resid[...].astype(jnp.float32)
    for piece, weight in zip(pieces, weights):
        mixed = mixed + jnp.dot(piece[...], weight[...], preferred_element_type=jnp.float32)
    mixed_out[...] = mixed
    factor = lax.rsqrt(jnp.mean(mixed * mixed, axis=1, keepdims=True) + EPS)
    normed_out[...] = (mixed * factor * gain[...]).astype(jnp.bfloat16)


def project(pieces, weights, resid, gain):
    return pl.pallas_call(
        functools.partial(project_kernel, len(pieces)),
        out_shape=(
            jax.ShapeDtypeStruct(resid.shape, jnp.float32),
            jax.ShapeDtypeStruct(resid.shape, jnp.bfloat16),
        ),
        name="project",
    )(*pieces, *weights, resid, gain)


def up_kernel(count, *refs):
    near, far = refs[:2]
    pieces = refs[2 : 2 + count]
    out, buf, acc, sems = refs[2 + count :]
    rows = near.shape[0]
    depth = pieces[0].shape[0]
    half = count // 2
    copies = [pltpu.make_async_copy(pieces[k], buf.at[k], sems.at[k]) for k in range(count)]
    for copy in copies:
        copy.start()
    for part in range(2):
        for k in range(part * half, (part + 1) * half):
            copies[k].wait()
        weight = buf[part * half : (part + 1) * half].reshape(half * depth, -1)
        for at, source in enumerate((near, far)):
            here = jnp.dot(
                source[:, part * half * depth : (part + 1) * half * depth],
                weight,
                preferred_element_type=jnp.float32,
            )
            span = slice(at * rows, (at + 1) * rows)
            if part == 0:
                acc[span] = here
            else:
                out[span] = jnp.square(jnp.maximum(acc[span] + here, 0.0)).astype(jnp.bfloat16)


def up_product(near, far, pieces):
    count = len(pieces)
    depth, width = pieces[0].shape
    total = 2 * near.shape[0]
    return pl.pallas_call(
        functools.partial(up_kernel, count),
        out_shape=jax.ShapeDtypeStruct((total, width), jnp.bfloat16),
        in_specs=[LOCAL, LOCAL] + [pl.BlockSpec(memory_space=pl.ANY)] * count,
        scratch_shapes=[
            pltpu.VMEM((count, depth, width), jnp.bfloat16),
            pltpu.VMEM((total, width), jnp.float32),
            pltpu.SemaphoreType.DMA((count,)),
        ],
        name="up",
    )(near, far, *pieces)


def tp_exchange(value):
    outer, a, c = places("tp")
    rows = value.shape[0] // (2 * outer)
    got = []
    for step in range(outer):
        for cross in range(2):
            to = 2 * ((a + step) % outer) + (c ^ cross)
            block = lax.dynamic_slice_in_dim(value, to * rows, rows, 0)
            if step or cross:
                block = shift(block, "tp", step, cross)
            got.append(block)
    return got


def tp_weights(value):
    outer = places("tp")[0]
    got = []
    for step in range(outer):
        here = shift(value, "tp", step) if step else value
        got += [here, flip(here, "tp")]
    return got


def tp_gather(value):
    outer = places("tp")[0]
    near = [value] + [shift(value, "tp", step) for step in range(1, outer)]
    near = jnp.concatenate(near, axis=0)
    return near, flip(near, "tp")


def tp_sum_back(parts, rows):
    outer = places("tp")[0]
    split = outer * rows
    paired = parts[:split].astype(jnp.float32) + flip(parts[split:], "tp").astype(jnp.float32)
    total = paired[:rows]
    for step in range(1, outer):
        block = paired[step * rows : (step + 1) * rows].astype(jnp.bfloat16)
        total = total + shift(block, "tp", outer - step).astype(jnp.float32)
    return total


def ring_shards(shard, hand_on):
    outer = places("sp")[0]
    here, got = shard, []
    for step in range(outer):
        if step:
            here = shift(here, "sp", 1)
        if hand_on and step and step == outer - 1:
            there = shift(got[-1][1], "sp", 1)
        else:
            there = flip(here, "sp")
        got.append((here, there))
    return got


def ring_sources():
    outer, a, c = places("sp")
    return [2 * ((a - step) % outer) + (c ^ cross) for step in range(outer) for cross in range(2)]


def shards(
    queries,
    keys,
    values,
    out_gate,
    input_gates,
    forget_gates,
    doc_ids,
    head_gain,
    w_out,
    resid,
    norm_gain,
    w_up,
    w_down,
):
    length = queries.shape[0]
    heads = input_gates.shape[1]
    outer, a, c = places("sp")
    up_ring = ring_shards(w_up, False)
    down_ring = ring_shards(w_down, True)
    out_shards = tp_weights(w_out)

    reach = min(2 * outer - 1, -(-(LONGEST_DOC - 1) // length))
    hops = min(outer - 1, -(-reach // 2))
    doc_pos = doc_ids.astype(jnp.float32)[None]
    info = jnp.stack([c, jnp.where(c == 1, a, outer - 1 - a)]).astype(jnp.int32)
    readouts = []
    for h in range(heads):
        cut = lambda x: x.reshape(length, heads, -1)[:, h]
        k, v = cut(keys), cut(values)
        gates = jnp.concatenate(
            [input_gates[:, h], forget_gates[:, h], doc_pos, jnp.zeros((3, length), jnp.float32)]
        )
        give, mine = summaries(info, k, v, gates)
        got = flip(give, "sp")
        pair = pair_state(mine, got)
        ahead = [carry_shift(pair, j) for j in range(1, hops + 1)]
        handed = flip(lead_state(info, ahead), "sp")
        readouts.append(
            emit(
                info,
                cut(queries),
                k,
                v,
                gates,
                cut(out_gate),
                head_gain.reshape(heads, 1, -1)[h],
                [got] + ahead,
                handed,
            )
        )
    readout = readouts[0] if heads == 1 else jnp.concatenate(readouts, axis=1)
    mixed, normed = project(tp_exchange(readout), out_shards, resid, norm_gain[None])

    rows = normed.shape[0]
    depth = w_up.shape[0]
    sources = ring_sources()
    turned = jnp.concatenate(
        [lax.dynamic_slice_in_dim(normed, at * depth, depth, 1) for at in sources], axis=1
    )
    near, far = tp_gather(turned)
    hidden = up_product(near, far, [shard for group in up_ring for shard in group])

    width = w_down.shape[1]
    out = jnp.zeros(resid.shape, jnp.bfloat16)
    for step, group in enumerate(down_ring):
        parts = []
        for shard in group:
            part = jnp.dot(hidden, shard, preferred_element_type=jnp.float32)
            parts.append(part.astype(jnp.bfloat16))
        parts = jnp.concatenate(parts, axis=1)
        summed = tp_sum_back(parts, rows)
        for cross in range(2):
            start = sources[2 * step + cross] * width
            piece = summed[:, cross * width : (cross + 1) * width]
            base = lax.dynamic_slice_in_dim(mixed, start, width, 1)
            out = lax.dynamic_update_slice_in_dim(
                out, (base + piece).astype(jnp.bfloat16), start, 1
            )
    return out


def solution(mesh):
    in_specs = (
        P("sp", "tp"),
        P("sp", "tp"),
        P("sp", "tp"),
        P("sp", "tp"),
        P(None, "tp", "sp"),
        P(None, "tp", "sp"),
        P("sp"),
        P("tp"),
        P("tp", None),
        P(("sp", "tp"), None),
        P(),
        P("sp", "tp"),
        P("tp", "sp"),
    )
    out_specs = P(("sp", "tp"), None)

    return jax.shard_map(shards, mesh=mesh, in_specs=in_specs, out_specs=out_specs, check_vma=False)
```

profile of v0, /device:TPU:0, one launch (start us, length us, event | category | flops | bytes accessed | tf_op | source)
XLA Modules:
  0.0 388.9 jit_solution(17332009834651707657)
XLA Ops:
  0.0 3.0 collective-permute-start.8
  3.0 45.8 %collective-permute-done.8.refs_6_ = bf16[512,2048]{1,0:T(8,128)(2,1)S(1)} collective-permute-done((bf16[512,2048]{1,0:T(8,128)(2,1)}, bf16[512,2048]{1,0:T(8,128)(2,1)S(1)}, u32[]{:S(2)}, u32[]{:S(2)}) %collective-permute-start.8) | collective-permute-done | bytes 2097184 | tf_op jit(solution)/shard_map/ppermute | solution.py:32
  48.8 0.7 pad_add_fusion.info
  49.6 0.7 convert_element_type.91
  50.3 0.7 copy_bitcast_fusion
  51.1 0.7 maximum_maximum_fusion.gates
  51.7 4.0 %summary.1 = (bf16[256,640]{1,0:T(8,128)(2,1)}, bf16[256,640]{1,0:T(8,128)(2,1)}) custom-call(s32[2]{0:T(128)} %pad_add_fusion.info, bf16[768,256]{1,0:T(8,128)(2,1)} %keys.3, bf16[768,512]{1,0:T(8,128)(2,1)} %values.3, f32[8,768]{1,0:T(8,128)} %maximum_maximum_fusion.gates), custom_call_target="tpu_custom_call" | custom-call | tf_op jit(solution)/shard_map/summary/pallas_call | solution.py:144
  55.8 1.8 collective-permute-start
  57.5 8.5 %collective-permute-done.got.rest_0_ = bf16[256,640]{1,0:T(8,128)(2,1)S(1)} collective-permute-done((bf16[256,640]{1,0:T(8,128)(2,1)}, bf16[256,640]{1,0:T(8,128)(2,1)S(1)}, u32[]{:S(2)}, u32[]{:S(2)}) %collective-permute-start) | collective-permute-done | bytes 327712 | tf_op jit(solution)/shard_map/ppermute | solution.py:24
  66.0 0.7 copy-done.7
  66.8 2.4 pair.1
  69.2 1.3 collective-permute-start.1
  70.5 2.7 collective-permute-start.13
  73.2 1.8 collective-permute-start.22
  75.0 5.5 %collective-permute-done.1.refs_0_.rest_1_ = bf16[256,640]{1,0:T(8,128)(2,1)S(1)} collective-permute-done((bf16[256,640]{1,0:T(8,128)(2,1)}, bf16[256,640]{1,0:T(8,128)(2,1)S(1)}, u32[]{:S(2)}, u32[]{:S(2)}) %collective-permute-start.1) | collective-permute-done | bytes 327712 | tf_op jit(solution)/shard_map/ppermute | solution.py:39
  80.5 1.3 collective-permute-start.2
  81.8 59.9 %collective-permute-done.2.refs_1_.rest_2_ = bf16[256,640]{1,0:T(8,128)(2,1)S(1)} collective-permute-done((bf16[256,640]{1,0:T(8,128)(2,1)}, bf16[256,640]{1,0:T(8,128)(2,1)S(1)}, u32[]{:S(2)}, u32[]{:S(2)}) %collective-permute-start.2) | collective-permute-done | bytes 327712 | tf_op jit(solution)/shard_map/ppermute | solution.py:39
  141.7 0.7 copy-done.6
  142.4 2.4 lead.1
  144.8 9.8 %collective-permute-done.3.rest_3_ = bf16[256,640]{1,0:T(8,128)(2,1)S(1)} collective-permute-done((bf16[256,640]{1,0:T(8,128)(2,1)}, bf16[256,640]{1,0:T(8,128)(2,1)S(1)}, u32[]{:S(2)}, u32[]{:S(2)}) %collective-permute-start.3) | collective-permute-done | bytes 327712 | tf_op jit(solution)/shard_map/ppermute | solution.py:24
  154.7 0.8 copy-done.14
  155.4 13.4 %emit.1 = bf16[768,512]{1,0:T(8,128)(2,1)} custom-call(s32[2]{0:T(128)} %pad_add_fusion.info, bf16[768,256]{1,0:T(8,128)(2,1)} %queries.1, bf16[768,256]{1,0:T(8,128)(2,1)} %keys.3, bf16[768,512]{1,0:T(8,128)(2,1)} %values.3, f32[8,768]{1,0:T(8,128)} %maximum_maximum_fusion.gates, bf16[768,512]{1,0:T(8,128)(2,1)} %out_gate.1, f32[1,512]{1,0:T(1,128)} %bitcast.25, ...), custom_call_target="tpu_custom_call" | custom-call | tf_op jit(solution)/shard_map/emit/pallas_call | solution.py:256
  168.8 2.0 constant_dynamic-slice_fusion
  170.8 1.5 collective-permute-start.5
  172.7 6.0 %collective-permute-done.5.refs_2_ = bf16[192,512]{1,0:T(8,128)(2,1)S(1)} collective-permute-done((bf16[192,512]{1,0:T(8,128)(2,1)S(1)}, bf16[192,512]{1,0:T(8,128)(2,1)S(1)}, u32[]{:S(2)}, u32[]{:S(2)}) %collective-permute-start.5) | collective-permute-done | bytes 196640 | tf_op jit(solution)/shard_map/ppermute | solution.py:32
  178.6 3.2 collective-permute-done.6.refs_3_
  181.8 0.6 copy-done.17
  182.5 7.1 %project.1 = (f32[192,2048]{1,0:T(8,128)}, bf16[192,2048]{1,0:T(8,128)(2,1)}) custom-call(bf16[192,512]{1,0:T(8,128)(2,1)} %get-tuple-element.16.refs_0_, bf16[192,512]{1,0:T(8,128)(2,1)} %copy-done.15, bf16[192,512]{1,0:T(8,128)(2,1)} %copy-done.16, bf16[192,512]{1,0:T(8,128)(2,1)} %copy-done.17, bf16[512,2048]{1,0:T(8,128)(2,1)} %refs_4_.1, ...), custom_call_target="tpu_custom_call" | custom-call | tf_op jit(solution)/shard_map/project/pallas_call | solution.py:296
  189.6 0.9 dynamic-slice_dynamic-update-slice_fusion.7
  190.5 0.9 dynamic-slice_dynamic-update-slice_fusion.6
  191.4 0.9 dynamic-slice_dynamic-update-slice_fusion.5
  192.3 0.9 dynamic-slice_dynamic-update-slice_fusion.4
  193.2 0.9 dynamic-slice_dynamic-update-slice_fusion.3
  194.1 0.9 dynamic-slice_dynamic-update-slice_fusion.2
  195.0 0.9 dynamic-slice_dynamic-update-slice_fusion.1
  195.9 0.9 dynamic-slice_dynamic-update-slice_fusion
  196.8 1.5 collective-permute-start.10
  198.6 2.2 collective-permute-done.15.refs_6_
  200.8 22.5 %collective-permute-done.26 = bf16[2048,256]{1,0:T(8,128)(2,1)} collective-permute-done((bf16[2048,256]{1,0:T(8,128)(2,1)}, bf16[2048,256]{1,0:T(8,128)(2,1)}, u32[]{:S(2)}, u32[]{:S(2)}) %collective-permute-start.26) | collective-permute-done | bytes 1048608 | tf_op jit(solution)/shard_map/ppermute | solution.py:32
  223.6 1.7 collective-permute-start.14
  225.9 19.1 %collective-permute-done.17.refs_8_ = bf16[256,2048]{1,0:T(8,128)(2,1)S(1)} collective-permute-done((bf16[256,2048]{1,0:T(8,128)(2,1)}, bf16[256,2048]{1,0:T(8,128)(2,1)S(1)}, u32[]{:S(2)}, u32[]{:S(2)}) %collective-permute-start.17) | collective-permute-done | bytes 1048608 | tf_op jit(solution)/shard_map/ppermute | solution.py:32
  245.3 4.3 %collective-permute-done.27 = bf16[2048,256]{1,0:T(8,128)(2,1)} collective-permute-done((bf16[2048,256]{1,0:T(8,128)(2,1)}, bf16[2048,256]{1,0:T(8,128)(2,1)}, u32[]{:S(2)}, u32[]{:S(2)}) %collective-permute-start.27) | collective-permute-done | bytes 1048608 | tf_op jit(solution)/shard_map/ppermute | solution.py:24
  249.6 22.4 %collective-permute-done.14.refs_5_ = bf16[256,2048]{1,0:T(8,128)(2,1)S(1)} collective-permute-done((bf16[256,2048]{1,0:T(8,128)(2,1)}, bf16[256,2048]{1,0:T(8,128)(2,1)S(1)}, u32[]{:S(2)}, u32[]{:S(2)}) %collective-permute-start.14) | collective-permute-done | bytes 1048608 | tf_op jit(solution)/shard_map/ppermute | solution.py:24
  272.0 22.5 %collective-permute-done.16.refs_7_ = bf16[256,2048]{1,0:T(8,128)(2,1)S(1)} collective-permute-done((bf16[256,2048]{1,0:T(8,128)(2,1)}, bf16[256,2048]{1,0:T(8,128)(2,1)S(1)}, u32[]{:S(2)}, u32[]{:S(2)}) %collective-permute-start.16) | collective-permute-done | bytes 1048608 | tf_op jit(solution)/shard_map/ppermute | solution.py:24
  294.8 22.2 %collective-permute-done.18.refs_9_ = bf16[256,2048]{1,0:T(8,128)(2,1)S(1)} collective-permute-done((bf16[256,2048]{1,0:T(8,128)(2,1)S(1)}, bf16[256,2048]{1,0:T(8,128)(2,1)S(1)}, u32[]{:S(2)}, u32[]{:S(2)}) %collective-permute-start.18) | collective-permute-done | bytes 1048608 | tf_op jit(solution)/shard_map/ppermute | solution.py:24
  317.2 0.7 copy-done.12
  317.9 1.2 copy-done.3
  319.1 12.5 %up.1 = bf16[768,2048]{1,0:T(8,128)(2,1)} custom-call(bf16[384,2048]{1,0:T(8,128)(2,1)} %copy-done, bf16[384,2048]{1,0:T(8,128)(2,1)} %copy-done.3, bf16[256,2048]{1,0:T(8,128)(2,1)} %refs_2_.1, bf16[256,2048]{1,0:T(8,128)(2,1)} %copy-done.8, bf16[256,2048]{1,0:T(8,128)(2,1)} %collective-permute-done.13.refs_4_, bf16[256,2048]{1,0:T(8,128)(2,1)} %copy-done.10, ...), custom_call_target="tpu_custom_call" | custom-call | tf_op jit(solution)/shard_map/up/pallas_call | solution.py:337
  331.6 3.3 convolution_convert_fusion
  334.9 2.2 convolution_convert_fusion.1
  337.3 2.2 convolution_convert_fusion.2
  339.5 2.2 convolution_convert_fusion.3
  342.3 2.2 convolution_convert_fusion.5
  344.5 15.4 %collective-permute-done.23 = bf16[2048,256]{1,0:T(8,128)(2,1)} collective-permute-done((bf16[2048,256]{1,0:T(8,128)(2,1)}, bf16[2048,256]{1,0:T(8,128)(2,1)}, u32[]{:S(2)}, u32[]{:S(2)}) %collective-permute-start.23) | collective-permute-done | bytes 1048608 | tf_op jit(solution)/shard_map/ppermute | solution.py:24
  359.9 2.2 convolution_convert_fusion.4
  362.2 2.2 convolution_convert_fusion.7
  364.4 2.2 convolution_convert_fusion.6
  367.4 1.6 collective-permute-start.33
  369.1 0.6 collective-permute-start.29
  369.9 1.6 collective-permute-start.21
  372.2 11.5 %collective-permute-done.21 = bf16[192,512]{1,0:T(8,128)(2,1)S(1)} collective-permute-done((bf16[192,512]{1,0:T(8,128)(2,1)S(1)}, bf16[192,512]{1,0:T(8,128)(2,1)S(1)}, u32[]{:S(2)}, u32[]{:S(2)}) %collective-permute-start.21) | collective-permute-done | bytes 196640 | tf_op jit(solution)/shard_map/ppermute | solution.py:32
  383.9 3.0 collective-permute-done.25
  387.4 0.9 copy-done.13
  388.2 0.7 fusion.19
  (96 shorter events, 5.6 us)
Async XLA Ops:
  0.0 48.8 %collective-permute-start.8 = (bf16[512,2048]{1,0:T(8,128)(2,1)}, bf16[512,2048]{1,0:T(8,128)(2,1)S(1)}, u32[]{:S(2)}, u32[]{:S(2)}) collective-permute-start(bf16[512,2048]{1,0:T(8,128)(2,1)} %refs_4_.1), channel_id=1, source_target_pairs={{0,2},{1,3},{2,0},{3,1},{4,6},{5,7},{6,4},{7,5},{8,10},{9,11},{10,... | collective-permute-start | bytes 6291464 | tf_op jit(solution)/shard_map/ppermute | solution.py:32
  3.0 178.8 %collective-permute-start.7 = (bf16[512,2048]{1,0:T(8,128)(2,1)}, bf16[512,2048]{1,0:T(8,128)(2,1)}, u32[]{:S(2)}, u32[]{:S(2)}) collective-permute-start(bf16[512,2048]{1,0:T(8,128)(2,1)} %refs_4_.1), channel_id=1, source_target_pairs={{0,1},{1,0},{2,3},{3,2},{4,5},{5,4},{6,7},{7,6},{8,9},{9,8},{10,11... | collective-permute-start | bytes 6291464 | tf_op jit(solution)/shard_map/ppermute | solution.py:24
  48.8 120.0 %copy-start.2 = (bf16[512,2048]{1,0:T(8,128)(2,1)}, bf16[512,2048]{1,0:T(8,128)(2,1)S(1)}, u32[]{:S(2)}) copy-start(bf16[512,2048]{1,0:T(8,128)(2,1)S(1)} %collective-permute-done.8.refs_6_) | copy-start | bytes 6291460
  48.8 133.0 %collective-permute-start.9 = (bf16[512,2048]{1,0:T(8,128)(2,1)S(1)}, bf16[512,2048]{1,0:T(8,128)(2,1)}, u32[]{:S(2)}, u32[]{:S(2)}) collective-permute-start(bf16[512,2048]{1,0:T(8,128)(2,1)S(1)} %collective-permute-done.8.refs_6_), channel_id=1, source_target_pairs={{0,1},{1,0},{2,3},{3,2},{4,5},{5,4},{6,7},{7,6},{8,9},{9,8},{10,11... | collective-permute-start | bytes 6291464 | tf_op jit(solution)/shard_map/ppermute | solution.py:24
  55.8 10.3 %collective-permute-start = (bf16[256,640]{1,0:T(8,128)(2,1)}, bf16[256,640]{1,0:T(8,128)(2,1)S(1)}, u32[]{:S(2)}, u32[]{:S(2)}) collective-permute-start(bf16[256,640]{1,0:T(8,128)(2,1)} %get-tuple-element.9), channel_id=1, source_target_pairs={{0,4},{4,0},{8,12},{12,8},{16,20},{20,16},{24,28},{28,24},{1,5},{5... | collective-permute-start | bytes 983048 | tf_op jit(solution)/shard_map/ppermute | solution.py:24
  66.0 0.7 copy-start.7
  69.2 11.3 %collective-permute-start.1 = (bf16[256,640]{1,0:T(8,128)(2,1)}, bf16[256,640]{1,0:T(8,128)(2,1)S(1)}, u32[]{:S(2)}, u32[]{:S(2)}) collective-permute-start(bf16[256,640]{1,0:T(8,128)(2,1)} %pair.1), channel_id=1, source_target_pairs={{8,0},{16,8},{24,16},{4,12},{12,20},{20,28},{9,1},{17,9},{25,17},{... | collective-permute-start | bytes 983048 | tf_op jit(solution)/shard_map/ppermute | solution.py:39
  70.5 100.3 %collective-permute-start.13 = (bf16[256,2048]{1,0:T(8,128)(2,1)}, bf16[256,2048]{1,0:T(8,128)(2,1)}, u32[]{:S(2)}, u32[]{:S(2)}) collective-permute-start(bf16[256,2048]{1,0:T(8,128)(2,1)} %refs_2_.1), channel_id=1, source_target_pairs={{0,8},{4,12},{8,16},{12,20},{16,24},{20,28},{24,0},{28,4},{1,9},{5... | collective-permute-start | bytes 3145736 | tf_op jit(solution)/shard_map/ppermute | solution.py:32
  73.2 99.2 %collective-permute-start.22 = (bf16[2048,256]{1,0:T(8,128)(2,1)}, bf16[2048,256]{1,0:T(8,128)(2,1)}, u32[]{:S(2)}, u32[]{:S(2)}) collective-permute-start(bf16[2048,256]{1,0:T(8,128)(2,1)} %param.25), channel_id=1, source_target_pairs={{0,8},{4,12},{8,16},{12,20},{16,24},{20,28},{24,0},{28,4},{1,9},{5... | collective-permute-start | bytes 3145736 | tf_op jit(solution)/shard_map/ppermute | solution.py:32
  80.5 61.2 %copy-start.5 = (bf16[256,640]{1,0:T(8,128)(2,1)}, bf16[256,640]{1,0:T(8,128)(2,1)S(1)}, u32[]{:S(2)}) copy-start(bf16[256,640]{1,0:T(8,128)(2,1)S(1)} %collective-permute-done.1.refs_0_.rest_1_) | copy-start | bytes 983044
  80.5 61.2 %collective-permute-start.2 = (bf16[256,640]{1,0:T(8,128)(2,1)}, bf16[256,640]{1,0:T(8,128)(2,1)S(1)}, u32[]{:S(2)}, u32[]{:S(2)}) collective-permute-start(bf16[256,640]{1,0:T(8,128)(2,1)} %pair.1), channel_id=1, source_target_pairs={{16,0},{24,8},{4,20},{12,28},{17,1},{25,9},{5,21},{13,29},{18,2},{... | collective-permute-start | bytes 983048 | tf_op jit(solution)/shard_map/ppermute | solution.py:39
  141.7 0.7 copy-start.6
  144.8 9.8 %collective-permute-start.3 = (bf16[256,640]{1,0:T(8,128)(2,1)}, bf16[256,640]{1,0:T(8,128)(2,1)S(1)}, u32[]{:S(2)}, u32[]{:S(2)}) collective-permute-start(bf16[256,640]{1,0:T(8,128)(2,1)} %lead.1), channel_id=1, source_target_pairs={{0,4},{4,0},{8,12},{12,8},{16,20},{20,16},{24,28},{28,24},{1,5},{5... | collective-permute-start | bytes 983048 | tf_op jit(solution)/shard_map/ppermute | solution.py:24
  154.7 0.8 copy-start.14
  170.8 1.9 collective-permute-start.4
  170.8 7.8 %collective-permute-start.5 = (bf16[192,512]{1,0:T(8,128)(2,1)S(1)}, bf16[192,512]{1,0:T(8,128)(2,1)S(1)}, u32[]{:S(2)}, u32[]{:S(2)}) collective-permute-start(bf16[192,512]{1,0:T(8,128)(2,1)S(1)} %get-tuple-element.14), channel_id=1, source_target_pairs={{0,2},{1,3},{2,0},{3,1},{4,6},{5,7},{6,4},{7,5},{8,10},{9,11},{10,... | collective-permute-start | bytes 589832 | tf_op jit(solution)/shard_map/ppermute | solution.py:32
  172.4 9.4 %collective-permute-start.6 = (bf16[192,512]{1,0:T(8,128)(2,1)S(1)}, bf16[192,512]{1,0:T(8,128)(2,1)S(1)}, u32[]{:S(2)}, u32[]{:S(2)}) collective-permute-start(bf16[192,512]{1,0:T(8,128)(2,1)S(1)} %get-tuple-element.13), channel_id=1, source_target_pairs={{0,3},{1,2},{2,1},{3,0},{4,7},{5,6},{6,5},{7,4},{8,11},{9,10},{10,... | collective-permute-start | bytes 589832 | tf_op jit(solution)/shard_map/ppermute | solution.py:32
  172.7 9.1 %copy-start.15 = (bf16[192,512]{1,0:T(8,128)(2,1)}, bf16[192,512]{1,0:T(8,128)(2,1)S(1)}, u32[]{:S(2)}) copy-start(bf16[192,512]{1,0:T(8,128)(2,1)S(1)} %collective-permute-done.4.refs_1_) | copy-start | bytes 589828
  172.7 28.1 %collective-permute-start.15 = (bf16[256,2048]{1,0:T(8,128)(2,1)}, bf16[256,2048]{1,0:T(8,128)(2,1)}, u32[]{:S(2)}, u32[]{:S(2)}) collective-permute-start(bf16[256,2048]{1,0:T(8,128)(2,1)} %collective-permute-done.13.refs_4_), channel_id=1, source_target_pairs={{0,8},{4,12},{8,16},{12,20},{16,24},{20,28},{24,0},{28,4},{1,9},{5... | collective-permute-start | bytes 3145736 | tf_op jit(solution)/shard_map/ppermute | solution.py:32
  178.6 3.2 copy-start.16
  178.6 44.6 %collective-permute-start.26 = (bf16[2048,256]{1,0:T(8,128)(2,1)}, bf16[2048,256]{1,0:T(8,128)(2,1)}, u32[]{:S(2)}, u32[]{:S(2)}) collective-permute-start(bf16[2048,256]{1,0:T(8,128)(2,1)} %collective-permute-done.22), channel_id=1, source_target_pairs={{0,8},{4,12},{8,16},{12,20},{16,24},{20,28},{24,0},{28,4},{1,9},{5... | collective-permute-start | bytes 3145736 | tf_op jit(solution)/shard_map/ppermute | solution.py:32
  181.8 0.7 copy-start.17
  196.8 28.5 %collective-permute-start.10 = (bf16[192,2048]{1,0:T(8,128)(2,1)S(1)}, bf16[192,2048]{1,0:T(8,128)(2,1)S(1)}, u32[]{:S(2)}, u32[]{:S(2)}) collective-permute-start(bf16[192,2048]{1,0:T(8,128)(2,1)S(1)} %dynamic-slice_dynamic-update-slice_fusion), channel_id=1, source_target_pairs={{0,2},{1,3},{2,0},{3,1},{4,6},{5,7},{6,4},{7,5},{8,10},{9,11},{10,... | collective-permute-start | bytes 2359304 | tf_op jit(solution)/shard_map/ppermute | solution.py:32
  198.3 27.2 %collective-permute-start.12 = (bf16[256,2048]{1,0:T(8,128)(2,1)}, bf16[256,2048]{1,0:T(8,128)(2,1)S(1)}, u32[]{:S(2)}, u32[]{:S(2)}) collective-permute-start(bf16[256,2048]{1,0:T(8,128)(2,1)} %refs_2_.1), channel_id=1, source_target_pairs={{0,4},{4,0},{8,12},{12,8},{16,20},{20,16},{24,28},{28,24},{1,5},{5... | collective-permute-start | bytes 3145736 | tf_op jit(solution)/shard_map/ppermute | solution.py:24
  200.8 44.2 %collective-permute-start.17 = (bf16[256,2048]{1,0:T(8,128)(2,1)}, bf16[256,2048]{1,0:T(8,128)(2,1)S(1)}, u32[]{:S(2)}, u32[]{:S(2)}) collective-permute-start(bf16[256,2048]{1,0:T(8,128)(2,1)} %collective-permute-done.15.refs_6_), channel_id=1, source_target_pairs={{0,8},{4,12},{8,16},{12,20},{16,24},{20,28},{24,0},{28,4},{1,9},{5... | collective-permute-start | bytes 3145736 | tf_op jit(solution)/shard_map/ppermute | solution.py:32
  223.3 26.3 %collective-permute-start.27 = (bf16[2048,256]{1,0:T(8,128)(2,1)}, bf16[2048,256]{1,0:T(8,128)(2,1)}, u32[]{:S(2)}, u32[]{:S(2)}) collective-permute-start(bf16[2048,256]{1,0:T(8,128)(2,1)} %collective-permute-done.26), channel_id=1, source_target_pairs={{0,4},{4,0},{8,12},{12,8},{16,20},{20,16},{24,28},{28,24},{1,5},{5... | collective-permute-start | bytes 3145736 | tf_op jit(solution)/shard_map/ppermute | solution.py:24
  223.6 48.4 %collective-permute-start.14 = (bf16[256,2048]{1,0:T(8,128)(2,1)}, bf16[256,2048]{1,0:T(8,128)(2,1)S(1)}, u32[]{:S(2)}, u32[]{:S(2)}) collective-permute-start(bf16[256,2048]{1,0:T(8,128)(2,1)} %collective-permute-done.13.refs_4_), channel_id=1, source_target_pairs={{0,4},{4,0},{8,12},{12,8},{16,20},{20,16},{24,28},{28,24},{1,5},{5... | collective-permute-start | bytes 3145736 | tf_op jit(solution)/shard_map/ppermute | solution.py:24
  225.4 92.5 %copy-start = (bf16[384,2048]{1,0:T(8,128)(2,1)}, bf16[384,2048]{1,0:T(8,128)(2,1)S(1)}, u32[]{:S(2)}) copy-start(bf16[384,2048]{1,0:T(8,128)(2,1)S(1)} %pad_maximum_fusion.refs_0_) | copy-start | bytes 4718596
  225.4 92.5 %collective-permute-start.11 = (bf16[384,2048]{1,0:T(8,128)(2,1)S(1)}, bf16[384,2048]{1,0:T(8,128)(2,1)S(1)}, u32[]{:S(2)}, u32[]{:S(2)}) collective-permute-start(bf16[384,2048]{1,0:T(8,128)(2,1)S(1)} %pad_maximum_fusion.refs_0_), channel_id=1, source_target_pairs={{0,1},{1,0},{2,3},{3,2},{4,5},{5,4},{6,7},{7,6},{8,9},{9,8},{10,11... | collective-permute-start | bytes 4718600 | tf_op jit(solution)/shard_map/ppermute | solution.py:24
  225.5 91.4 %copy-start.8 = (bf16[256,2048]{1,0:T(8,128)(2,1)}, bf16[256,2048]{1,0:T(8,128)(2,1)S(1)}, u32[]{:S(2)}) copy-start(bf16[256,2048]{1,0:T(8,128)(2,1)S(1)} %collective-permute-done.12.refs_3_) | copy-start | bytes 3145732
  225.5 68.9 %collective-permute-start.16 = (bf16[256,2048]{1,0:T(8,128)(2,1)}, bf16[256,2048]{1,0:T(8,128)(2,1)S(1)}, u32[]{:S(2)}, u32[]{:S(2)}) collective-permute-start(bf16[256,2048]{1,0:T(8,128)(2,1)} %collective-permute-done.15.refs_6_), channel_id=1, source_target_pairs={{0,4},{4,0},{8,12},{12,8},{16,20},{20,16},{24,28},{28,24},{1,5},{5... | collective-permute-start | bytes 3145736 | tf_op jit(solution)/shard_map/ppermute | solution.py:24
  245.0 72.2 %copy-start.9 = (bf16[256,2048]{1,0:T(8,128)(2,1)}, bf16[256,2048]{1,0:T(8,128)(2,1)S(1)}, u32[]{:S(2)}) copy-start(bf16[256,2048]{1,0:T(8,128)(2,1)S(1)} %collective-permute-done.17.refs_8_) | copy-start | bytes 3145732
  245.0 71.9 %collective-permute-start.18 = (bf16[256,2048]{1,0:T(8,128)(2,1)S(1)}, bf16[256,2048]{1,0:T(8,128)(2,1)S(1)}, u32[]{:S(2)}, u32[]{:S(2)}) collective-permute-start(bf16[256,2048]{1,0:T(8,128)(2,1)S(1)} %collective-permute-done.17.refs_8_), channel_id=1, source_target_pairs={{0,4},{4,0},{8,12},{12,8},{16,20},{20,16},{24,28},{28,24},{1,5},{5... | collective-permute-start | bytes 3145736 | tf_op jit(solution)/shard_map/ppermute | solution.py:24
  249.6 82.0 %collective-permute-start.31 = (bf16[2048,256]{1,0:T(8,128)(2,1)}, bf16[2048,256]{1,0:T(8,128)(2,1)}, u32[]{:S(2)}, u32[]{:S(2)}) collective-permute-start(bf16[2048,256]{1,0:T(8,128)(2,1)} %collective-permute-done.27), channel_id=1, source_target_pairs={{0,8},{4,12},{8,16},{12,20},{16,24},{20,28},{24,0},{28,4},{1,9},{5... | collective-permute-start | bytes 3145736 | tf_op jit(solution)/shard_map/ppermute | solution.py:32
  272.0 45.2 %copy-start.10 = (bf16[256,2048]{1,0:T(8,128)(2,1)}, bf16[256,2048]{1,0:T(8,128)(2,1)S(1)}, u32[]{:S(2)}) copy-start(bf16[256,2048]{1,0:T(8,128)(2,1)S(1)} %collective-permute-done.14.refs_5_) | copy-start | bytes 3145732
  272.0 62.9 %collective-permute-start.30 = (bf16[2048,256]{1,0:T(8,128)(2,1)}, bf16[2048,256]{1,0:T(8,128)(2,1)}, u32[]{:S(2)}, u32[]{:S(2)}) collective-permute-start(bf16[2048,256]{1,0:T(8,128)(2,1)} %collective-permute-done.26), channel_id=1, source_target_pairs={{0,8},{4,12},{8,16},{12,20},{16,24},{20,28},{24,0},{28,4},{1,9},{5... | collective-permute-start | bytes 3145736 | tf_op jit(solution)/shard_map/ppermute | solution.py:32
  294.5 22.8 %copy-start.11 = (bf16[256,2048]{1,0:T(8,128)(2,1)}, bf16[256,2048]{1,0:T(8,128)(2,1)S(1)}, u32[]{:S(2)}) copy-start(bf16[256,2048]{1,0:T(8,128)(2,1)S(1)} %collective-permute-done.16.refs_7_) | copy-start | bytes 3145732
  294.5 70.0 %collective-permute-start.19 = (bf16[2048,256]{1,0:T(8,128)(2,1)}, bf16[2048,256]{1,0:T(8,128)(2,1)}, u32[]{:S(2)}, u32[]{:S(2)}) collective-permute-start(bf16[2048,256]{1,0:T(8,128)(2,1)} %param.25), channel_id=1, source_target_pairs={{0,4},{4,0},{8,12},{12,8},{16,20},{20,16},{24,28},{28,24},{1,5},{5... | collective-permute-start | bytes 3145736 | tf_op jit(solution)/shard_map/ppermute | solution.py:24
  316.9 1.0 copy-start.12
  316.9 42.9 %collective-permute-start.23 = (bf16[2048,256]{1,0:T(8,128)(2,1)}, bf16[2048,256]{1,0:T(8,128)(2,1)}, u32[]{:S(2)}, u32[]{:S(2)}) collective-permute-start(bf16[2048,256]{1,0:T(8,128)(2,1)} %collective-permute-done.22), channel_id=1, source_target_pairs={{0,4},{4,0},{8,12},{12,8},{16,20},{20,16},{24,28},{28,24},{1,5},{5... | collective-permute-start | bytes 3145736 | tf_op jit(solution)/shard_map/ppermute | solution.py:24
  317.9 1.2 copy-start.3
  331.6 3.3 copy-start.1
  337.2 30.1 %collective-permute-start.32 = (bf16[384,512]{1,0:T(8,128)(2,1)S(1)}, bf16[384,512]{1,0:T(8,128)(2,1)S(1)}, u32[]{:S(2)}, u32[]{:S(2)}) collective-permute-start(bf16[384,512]{1,0:T(8,128)(2,1)S(1)} %pad_maximum_fusion.1), channel_id=1, source_target_pairs={{0,1},{1,0},{2,3},{3,2},{4,5},{5,4},{6,7},{7,6},{8,9},{9,8},{10,11... | collective-permute-start | bytes 1179656 | tf_op jit(solution)/shard_map/ppermute | solution.py:24
  341.7 27.2 %collective-permute-start.28 = (bf16[384,512]{1,0:T(8,128)(2,1)S(1)}, bf16[384,512]{1,0:T(8,128)(2,1)S(1)}, u32[]{:S(2)}, u32[]{:S(2)}) collective-permute-start(bf16[384,512]{1,0:T(8,128)(2,1)S(1)} %pad_maximum_fusion.2), channel_id=1, source_target_pairs={{0,1},{1,0},{2,3},{3,2},{4,5},{5,4},{6,7},{7,6},{8,9},{9,8},{10,11... | collective-permute-start | bytes 1179656 | tf_op jit(solution)/shard_map/ppermute | solution.py:24
  362.1 9.3 %collective-permute-start.24 = (bf16[384,512]{1,0:T(8,128)(2,1)S(1)}, bf16[384,512]{1,0:T(8,128)(2,1)S(1)}, u32[]{:S(2)}, u32[]{:S(2)}) collective-permute-start(bf16[384,512]{1,0:T(8,128)(2,1)S(1)} %pad_maximum_fusion.3), channel_id=1, source_target_pairs={{0,1},{1,0},{2,3},{3,2},{4,5},{5,4},{6,7},{7,6},{8,9},{9,8},{10,11... | collective-permute-start | bytes 1179656 | tf_op jit(solution)/shard_map/ppermute | solution.py:24
  366.7 3.0 collective-permute-start.20
  367.4 19.8 %collective-permute-start.33 = (bf16[192,512]{1,0:T(8,128)(2,1)S(1)}, bf16[192,512]{1,0:T(8,128)(2,1)S(1)}, u32[]{:S(2)}, u32[]{:S(2)}) collective-permute-start(bf16[192,512]{1,0:T(8,128)(2,1)S(1)} %slice.204), channel_id=1, source_target_pairs={{0,2},{1,3},{2,0},{3,1},{4,6},{5,7},{6,4},{7,5},{8,10},{9,11},{10,... | collective-permute-start | bytes 589832 | tf_op jit(solution)/shard_map/ppermute | solution.py:32
  369.1 14.7 %copy-start.4 = (f32[192,2048]{1,0:T(8,128)S(1)}, f32[192,2048]{1,0:T(8,128)}, u32[]{:S(2)}) copy-start(f32[192,2048]{1,0:T(8,128)} %get-tuple-element.11) | copy-start | bytes 4718596
  369.1 18.0 %collective-permute-start.29 = (bf16[192,512]{1,0:T(8,128)(2,1)S(1)}, bf16[192,512]{1,0:T(8,128)(2,1)S(1)}, u32[]{:S(2)}, u32[]{:S(2)}) collective-permute-start(bf16[192,512]{1,0:T(8,128)(2,1)S(1)} %slice.205), channel_id=1, source_target_pairs={{0,2},{1,3},{2,0},{3,1},{4,6},{5,7},{6,4},{7,5},{8,10},{9,11},{10,... | collective-permute-start | bytes 589832 | tf_op jit(solution)/shard_map/ppermute | solution.py:32
  369.9 13.8 %collective-permute-start.21 = (bf16[192,512]{1,0:T(8,128)(2,1)S(1)}, bf16[192,512]{1,0:T(8,128)(2,1)S(1)}, u32[]{:S(2)}, u32[]{:S(2)}) collective-permute-start(bf16[192,512]{1,0:T(8,128)(2,1)S(1)} %slice.207), channel_id=1, source_target_pairs={{0,2},{1,3},{2,0},{3,1},{4,6},{5,7},{6,4},{7,5},{8,10},{9,11},{10,... | collective-permute-start | bytes 589832 | tf_op jit(solution)/shard_map/ppermute | solution.py:32
  371.6 15.3 %collective-permute-start.25 = (bf16[192,512]{1,0:T(8,128)(2,1)S(1)}, bf16[192,512]{1,0:T(8,128)(2,1)S(1)}, u32[]{:S(2)}, u32[]{:S(2)}) collective-permute-start(bf16[192,512]{1,0:T(8,128)(2,1)S(1)} %slice.206), channel_id=1, source_target_pairs={{0,2},{1,3},{2,0},{3,1},{4,6},{5,7},{6,4},{7,5},{8,10},{9,11},{10,... | collective-permute-start | bytes 589832 | tf_op jit(solution)/shard_map/ppermute | solution.py:32
  387.4 0.9 copy-start.13
where the time goes:
time: 390 us; the launch traced here: 389 us
  waiting for transfers between devices  284 us (73%)
  Pallas kernels  41.9 us (11%)
  starting transfers between devices  24.3 us (6%)
  matrix products  18.8 us (5%)
  local copies, waits for them, and re-layouts  15.8 us (4%)
  other arithmetic  3.92 us (1%)
    ppermute x16, waiting for transfers between devices, shift(): return lax.ppermute(value, axis, moves)  113 us
    ppermute x16, waiting for transfers between devices, flip(): lax.ppermute(value, axis, [(i, i ^ 1) for i in range(lax.axis_size(axis))])  105 us
    ppermute x2, waiting for transfers between devices, carry_shift(): return lax.ppermute(value, 'sp', moves)  65.4 us
    dot_general x8, matrix products, shards(): part = jnp.dot(hidden, shard, preferred_element_type=jnp.float32)  18.8 us
    ppermute x16, starting transfers between devices, shift(): return lax.ppermute(value, axis, moves)  15.1 us
    pallas_call x1, Pallas kernels, emit(): pl.pallas_call(functools.partial(emit_kernel, len(states) - 1), out_shape...  13.4 us
    unnamed x44, local copies, waits for them, and re-layouts  12.7 us
    pallas_call x1, Pallas kernels, up_product(): pl.pallas_call(functools.partial(up_kernel, count), out_shape=jax.ShapeDt...  12.5 us
  transfers between devices with their start and end apart: 34, of which 17 were waited for; matrix products, arithmetic and copies ran while one was open for 8% of the time, Pallas kernels for 11%

commit v1 on v0

--- a/solution.py
+++ b/solution.py
@@ -10,7 +10,8 @@
 EPS = 1e-06
 FAR_LOW = -1e30
 LONGEST_DOC = 3072
-EXTRA = 128
+LANES = 128
+EXTRA = LANES
 
 
 def places(axis):
@@ -30,6 +31,11 @@
         (2 * a + c, 2 * ((a + step) % outer) + (c ^ cross)) for a in range(outer) for c in range(2)
     ]
     return lax.ppermute(value, axis, moves)
+
+
+def neighbour(value):
+    moves = [(i, i ^ 2) for i in range(lax.axis_size("sp"))]
+    return lax.ppermute(value, "sp", moves)
 
 
 def carry_shift(value, step):
@@ -281,33 +287,52 @@
     )(info, queries, keys, values, gates, out_gate, gain, *states, handed)
 
 
-def project_kernel(count, *refs):
+def project_kernel(count, turn, info, *refs):
     pieces, weights = refs[:count], refs[count : 2 * count]
-    resid, gain, mixed_out, normed_out = refs[2 * count :]
+    resid, gain, mixed_out, normed_out, beside_out, whole = refs[2 * count :]
     mixed = resid[...].astype(jnp.float32)
     for piece, weight in zip(pieces, weights):
         mixed = mixed + jnp.dot(piece[...], weight[...], preferred_element_type=jnp.float32)
     mixed_out[...] = mixed
     factor = lax.rsqrt(jnp.mean(mixed * mixed, axis=1, keepdims=True) + EPS)
-    normed_out[...] = (mixed * factor * gain[...]).astype(jnp.bfloat16)
-
-
-def project(pieces, weights, resid, gain):
-    return pl.pallas_call(
-        functools.partial(project_kernel, len(pieces)),
+    normed = mixed * factor * gain[...]
+    if not turn:
+        normed_out[...] = normed.astype(jnp.bfloat16)
+        beside_out[...] = normed_out[...]
+        return
+    whole[...] = normed
+    depth = mixed.shape[1] // turn
+    for k in range(turn):
+        at = pl.multiple_of(info[k] * depth, LANES)
+        part = whole[:, pl.ds(at, depth)].astype(jnp.bfloat16)
+        normed_out[:, k * depth : (k + 1) * depth] = part
+        beside_out[:, (k ^ 1) * depth : ((k ^ 1) + 1) * depth] = part
+
+
+def project(pieces, weights, resid, gain, sources, depth):
+    inside = depth % LANES == 0
+    mixed, normed, beside = pl.pallas_call(
+        functools.partial(project_kernel, len(pieces), len(sources) if inside else 0),
         out_shape=(
             jax.ShapeDtypeStruct(resid.shape, jnp.float32),
             jax.ShapeDtypeStruct(resid.shape, jnp.bfloat16),
+            jax.ShapeDtypeStruct(resid.shape, jnp.bfloat16),
         ),
+        in_specs=[SMALL] + [LOCAL] * (2 * len(pieces) + 2),
+        scratch_shapes=[pltpu.VMEM(resid.shape, jnp.float32)],
         name="project",
-    )(*pieces, *weights, resid, gain)
-
-
-def up_kernel(count, *refs):
-    near, far = refs[:2]
-    pieces = refs[2 : 2 + count]
-    out, buf, acc, sems = refs[2 + count :]
-    rows = near.shape[0]
+    )(jnp.stack(sources).astype(jnp.int32), *pieces, *weights, resid, gain)
+    if not inside:
+        cuts = [lax.dynamic_slice_in_dim(normed, at * depth, depth, 1) for at in sources]
+        normed = jnp.concatenate(cuts, axis=1)
+        beside = jnp.concatenate([cuts[k ^ 1] for k in range(len(cuts))], axis=1)
+    return mixed, normed, beside
+
+
+def up_kernel(blocks, count, *refs):
+    rows = refs[:blocks]
+    pieces = refs[blocks : blocks + count]
+    out, buf, acc, sems = refs[blocks + count :]
     depth = pieces[0].shape[0]
     half = count // 2
     copies = [pltpu.make_async_copy(pieces[k], buf.at[k], sems.at[k]) for k in range(count)]
@@ -317,34 +342,59 @@
         for k in range(part * half, (part + 1) * half):
             copies[k].wait()
         weight = buf[part * half : (part + 1) * half].reshape(half * depth, -1)
-        for at, source in enumerate((near, far)):
+        at = 0
+        for source in rows:
             here = jnp.dot(
                 source[:, part * half * depth : (part + 1) * half * depth],
                 weight,
                 preferred_element_type=jnp.float32,
             )
-            span = slice(at * rows, (at + 1) * rows)
+            span = slice(at, at + source.shape[0])
+            at += source.shape[0]
             if part == 0:
                 acc[span] = here
             else:
                 out[span] = jnp.square(jnp.maximum(acc[span] + here, 0.0)).astype(jnp.bfloat16)
 
 
-def up_product(near, far, pieces):
+def up_product(rows, pieces):
     count = len(pieces)
     depth, width = pieces[0].shape
-    total = 2 * near.shape[0]
+    total = sum(r.shape[0] for r in rows)
     return pl.pallas_call(
-        functools.partial(up_kernel, count),
+        functools.partial(up_kernel, len(rows), count),
         out_shape=jax.ShapeDtypeStruct((total, width), jnp.bfloat16),
-        in_specs=[LOCAL, LOCAL] + [pl.BlockSpec(memory_space=pl.ANY)] * count,
+        in_specs=[LOCAL] * len(rows) + [pl.BlockSpec(memory_space=pl.ANY)] * count,
         scratch_shapes=[
             pltpu.VMEM((count, depth, width), jnp.bfloat16),
             pltpu.VMEM((total, width), jnp.float32),
             pltpu.SemaphoreType.DMA((count,)),
         ],
-        name="up",
-    )(near, far, *pieces)
+    )(*rows, *pieces)
+
+
+def down_kernel(early, late, *refs):
+    pieces, (near, far) = refs[:-2], refs[-2:]
+    at = 0
+    for piece in pieces:
+        cols = slice(at, at + piece.shape[1])
+        at += piece.shape[1]
+        for place, out in enumerate((near, far)):
+            top = 0
+            for hidden in (early, late):
+                rows = hidden.shape[0] // 2
+                out[top : top + rows, cols] = jnp.dot(
+                    hidden[place * rows : (place + 1) * rows],
+                    piece[...],
+                    preferred_element_type=jnp.float32,
+                ).astype(jnp.bfloat16)
+                top += rows
+
+
+def down_product(early, late, pieces):
+    rows = (early.shape[0] + late.shape[0]) // 2
+    shape = jax.ShapeDtypeStruct((rows, sum(p.shape[1] for p in pieces)), jnp.bfloat16)
+    return pl.pallas_call(down_kernel, out_shape=(shape, shape))(early, late, *pieces)
 
 
 def tp_exchange(value):
@@ -370,41 +420,63 @@
     return got
 
 
-def tp_gather(value):
+def row_blocks(value, given):
     outer = places("tp")[0]
-    near = [value] + [shift(value, "tp", step) for step in range(1, outer)]
-    near = jnp.concatenate(near, axis=0)
-    return near, flip(near, "tp")
-
-
-def tp_sum_back(parts, rows):
+    beside = neighbour(given)
+    across = [shift(value, "tp", step) for step in range(1, outer)]
+    late = [shift(beside, "tp", step) for step in range(1, outer)]
+    second = jnp.concatenate([beside] + across, axis=0)
+    third = late[0] if len(late) == 1 else jnp.concatenate(late, axis=0)
+    return (value, second), (third,), (flip(value, "tp"), flip(second, "tp"), flip(third, "tp"))
+
+
+def sum_back(near, far, rows, line_first):
     outer = places("tp")[0]
-    split = outer * rows
-    paired = parts[:split].astype(jnp.float32) + flip(parts[split:], "tp").astype(jnp.float32)
-    total = paired[:rows]
+    paired = near.astype(jnp.float32) + flip(far, "tp").astype(jnp.float32)
+    block = lambda k: paired[k * rows : (k + 1) * rows]
+    send = lambda blocks: jnp.concatenate(blocks, axis=0).astype(jnp.bfloat16)
+    own = [block(0)] + [block(1 + step) for step in range(1, outer)]
+    beside = [block(1)] + [block(outer + step) for step in range(1, outer)]
+    turned = lambda x: jnp.concatenate([x[:, x.shape[1] // 2 :], x[:, : x.shape[1] // 2]], axis=1)
+    if line_first:
+        got = neighbour(turned(send(beside))).astype(jnp.float32)
+        own = [b + got[k * rows : (k + 1) * rows] for k, b in enumerate(own)]
+        total = own[0]
+        for step in range(1, outer):
+            block_sent = own[step].astype(jnp.bfloat16)
+            total = total + shift(block_sent, "tp", outer - step).astype(jnp.float32)
+        return total
+    total, other = own[0], beside[0]
     for step in range(1, outer):
-        block = paired[step * rows : (step + 1) * rows].astype(jnp.bfloat16)
-        total = total + shift(block, "tp", outer - step).astype(jnp.float32)
-    return total
-
-
-def ring_shards(shard, hand_on):
-    outer = places("sp")[0]
-    here, got = shard, []
-    for step in range(outer):
+        got = shift(send([own[step], beside[step]]), "tp", outer - step)
+        total = total + got[:rows].astype(jnp.float32)
+        other = other + got[rows:].astype(jnp.float32)
+    other = turned(other.astype(jnp.bfloat16))
+    return total + neighbour(other).astype(jnp.float32)
+
+
+def half_shards(shard, dim):
+    outer, a, _ = places("sp")
+    size = shard.shape[dim] // 2
+    kept = lax.dynamic_slice_in_dim(shard, (a % 2) * size, size, dim)
+    given = lax.dynamic_slice_in_dim(shard, (1 - a % 2) * size, size, dim)
+    here, got = [kept, neighbour(given)], []
+    for step in range(outer // 2):
         if step:
-            here = shift(here, "sp", 1)
-        if hand_on and step and step == outer - 1:
-            there = shift(got[-1][1], "sp", 1)
-        else:
-            there = flip(here, "sp")
-        got.append((here, there))
+            here = [shift(x, "sp", 2) for x in here]
+        got += [here, [flip(x, "sp") for x in here]]
     return got
 
 
 def ring_sources():
     outer, a, c = places("sp")
-    return [2 * ((a - step) % outer) + (c ^ cross) for step in range(outer) for cross in range(2)]
+    assert outer % 2 == 0
+    return [
+        2 * (((a - 2 * step) % outer) ^ k) + (c ^ cross)
+        for step in range(outer // 2)
+        for cross in range(2)
+        for k in range(2)
+    ]
 
 
 def shards(
@@ -425,8 +497,8 @@
     length = queries.shape[0]
     heads = input_gates.shape[1]
     outer, a, c = places("sp")
-    up_ring = ring_shards(w_up, False)
-    down_ring = ring_shards(w_down, True)
+    up_ring = half_shards(w_up, 1)
+    down_ring = half_shards(w_down, 0)
     out_shards = tp_weights(w_out)
 
     reach = min(2 * outer - 1, -(-(LONGEST_DOC - 1) // length))
@@ -459,29 +531,24 @@
             )
         )
     readout = readouts[0] if heads == 1 else jnp.concatenate(readouts, axis=1)
-    mixed, normed = project(tp_exchange(readout), out_shards, resid, norm_gain[None])
-
+    sources = ring_sources()
+    mixed, normed, given = project(
+        tp_exchange(readout), out_shards, resid, norm_gain[None], sources, w_up.shape[0]
+    )
     rows = normed.shape[0]
-    depth = w_up.shape[0]
-    sources = ring_sources()
-    turned = jnp.concatenate(
-        [lax.dynamic_slice_in_dim(normed, at * depth, depth, 1) for at in sources], axis=1
-    )
-    near, far = tp_gather(turned)
-    hidden = up_product(near, far, [shard for group in up_ring for shard in group])
+    early, late, partner = row_blocks(normed, given)
+    up_pieces = [shard for group in up_ring for shard in group]
+    early = up_product([*early, *partner[:2]], up_pieces)
+    late = up_product([*late, partner[2]], up_pieces)
 
     width = w_down.shape[1]
     out = jnp.zeros(resid.shape, jnp.bfloat16)
     for step, group in enumerate(down_ring):
-        parts = []
-        for shard in group:
-            part = jnp.dot(hidden, shard, preferred_element_type=jnp.float32)
-            parts.append(part.astype(jnp.bfloat16))
-        parts = jnp.concatenate(parts, axis=1)
-        summed = tp_sum_back(parts, rows)
-        for cross in range(2):
-            start = sources[2 * step + cross] * width
-            piece = summed[:, cross * width : (cross + 1) * width]
+        near, far = down_product(early, late, group)
+        summed = sum_back(near, far, rows, step % 2 == 1)
+        for k in range(2):
+            start = sources[2 * step + k] * width
+            piece = summed[:, k * width : (k + 1) * width]
             base = lax.dynamic_slice_in_dim(mixed, start, width, 1)
             out = lax.dynamic_update_slice_in_dim(
                 out, (base + piece).astype(jnp.bfloat16), start, 1

time: 390 us -> 355 us (0.910)
  waiting for transfers between devices: 284 us -> 233 us
  Pallas kernels: 41.9 us -> 66.4 us
  matrix products: 18.8 us -> 0 us
  starting transfers between devices: 24.3 us -> 36.9 us
  local copies, waits for them, and re-layouts: 15.8 us -> 11.9 us
    ppermute x16 -> x19, waiting for transfers between devices: 105 us -> 42.6 us  [flip(): lax.ppermute(value, axis, [(i, i ^ 1) for i in range(lax.axis_size(axis))])]
    ppermute x0 -> x7, waiting for transfers between devices: none -> 59.9 us  [neighbour(): return lax.ppermute(value, 'sp', moves)]
    ppermute x2, waiting for transfers between devices: 65.4 us -> 24 us  [carry_shift(): return lax.ppermute(value, 'sp', moves)]
    pallas_call x2 -> x7, Pallas kernels: 19.6 us -> 44.1 us  [the longest x4 20.1 us: down_product(): pl.pallas_call(down_kernel, out_shape=(shape, shape))(early, late, *pieces)]
    dot_general x8 -> x0, matrix products: 18.8 us -> none  [shards(): part = jnp.dot(hidden, shard, preferred_element_type=jnp.float32)]
    ppermute x16 -> x14, waiting for transfers between devices: 113 us -> 106 us  [shift(): return lax.ppermute(value, axis, moves)]
    ppermute x16 -> x19, starting transfers between devices: 6.63 us -> 12.6 us  [flip(): lax.ppermute(value, axis, [(i, i ^ 1) for i in range(lax.axis_size(axis))])]
    unnamed x44 -> x68, local copies, waits for them, and re-layouts: 12.7 us -> 7.63 us
  transfers between devices with their start and end apart: 34 -> 42, of which waited for: 17 -> 19; matrix products, arithmetic and copies ran while one was open for 8% -> 3% of each run, Pallas kernels for 11% -> 15%
where the time goes in v1:
time: 355 us; the launch traced here: 354 us
  waiting for transfers between devices  233 us (66%)
  Pallas kernels  66.4 us (19%)
  starting transfers between devices  36.9 us (10%)
  local copies, waits for them, and re-layouts  11.9 us (3%)
  other arithmetic  5.87 us (2%)
    ppermute x14, waiting for transfers between devices, shift(): return lax.ppermute(value, axis, moves)  106 us
    ppermute x7, waiting for transfers between devices, neighbour(): return lax.ppermute(value, 'sp', moves)  59.9 us
    ppermute x19, waiting for transfers between devices, flip(): lax.ppermute(value, axis, [(i, i ^ 1) for i in range(lax.axis_size(axis))])  42.6 us
    ppermute x2, waiting for transfers between devices, carry_shift(): return lax.ppermute(value, 'sp', moves)  24 us
    pallas_call x4, Pallas kernels, down_product(): pl.pallas_call(down_kernel, out_shape=(shape, shape))(early, late, *pieces)  20.1 us
    ppermute x14, starting transfers between devices, shift(): return lax.ppermute(value, axis, moves)  18.6 us
    pallas_call x2, Pallas kernels, up_product(): pl.pallas_call(functools.partial(up_kernel, len(rows), count), out_shape=...  16.3 us
    pallas_call x1, Pallas kernels, emit(): pl.pallas_call(functools.partial(emit_kernel, len(states) - 1), out_shape...  13.4 us
  transfers between devices with their start and end apart: 42, of which 19 were waited for; matrix products, arithmetic and copies ran while one was open for 3% of the time, Pallas kernels for 15%

profile of v1, /device:TPU:0, one launch (start us, length us, event | category | flops | bytes accessed | tf_op | source)
XLA Modules:
  0.0 354.2 jit_solution(5488451725789567668)
XLA Ops:
  0.0 3.0 collective-permute-start.8
  3.0 45.8 %collective-permute-done.8.refs_6_ = bf16[512,2048]{1,0:T(8,128)(2,1)S(1)} collective-permute-done((bf16[512,2048]{1,0:T(8,128)(2,1)}, bf16[512,2048]{1,0:T(8,128)(2,1)S(1)}, u32[]{:S(2)}, u32[]{:S(2)}) %collective-permute-start.8) | collective-permute-done | bytes 2097184 | tf_op jit(solution)/shard_map/ppermute | solution.py:33
  50.2 0.7 copy_bitcast_fusion
  51.6 4.0 %summary.1 = (bf16[256,640]{1,0:T(8,128)(2,1)}, bf16[256,640]{1,0:T(8,128)(2,1)}) custom-call(s32[2]{0:T(128)} %pad_add_fusion.info, bf16[768,256]{1,0:T(8,128)(2,1)} %keys.3, bf16[768,512]{1,0:T(8,128)(2,1)} %values.3, f32[8,768]{1,0:T(8,128)} %maximum_maximum_fusion.gates), custom_call_target="tpu_custom_call" | custom-call | tf_op jit(solution)/shard_map/summary/pallas_call | solution.py:150
  55.6 1.8 collective-permute-start
  57.4 8.6 %collective-permute-done.got.rest_0_ = bf16[256,640]{1,0:T(8,128)(2,1)S(1)} collective-permute-done((bf16[256,640]{1,0:T(8,128)(2,1)}, bf16[256,640]{1,0:T(8,128)(2,1)S(1)}, u32[]{:S(2)}, u32[]{:S(2)}) %collective-permute-start) | collective-permute-done | bytes 327712 | tf_op jit(solution)/shard_map/ppermute | solution.py:25
  66.0 0.7 copy-done.15
  66.7 2.4 pair.1
  69.1 1.3 collective-permute-start.1
  70.4 1.3 collective-permute-start.2
  71.7 9.0 %collective-permute-done.1.refs_0_.rest_1_ = bf16[256,640]{1,0:T(8,128)(2,1)S(1)} collective-permute-done((bf16[256,640]{1,0:T(8,128)(2,1)}, bf16[256,640]{1,0:T(8,128)(2,1)S(1)}, u32[]{:S(2)}, u32[]{:S(2)}) %collective-permute-start.1) | collective-permute-done | bytes 327712 | tf_op jit(solution)/shard_map/ppermute | solution.py:45
  80.7 15.1 %collective-permute-done.2.refs_1_.rest_2_ = bf16[256,640]{1,0:T(8,128)(2,1)S(1)} collective-permute-done((bf16[256,640]{1,0:T(8,128)(2,1)}, bf16[256,640]{1,0:T(8,128)(2,1)S(1)}, u32[]{:S(2)}, u32[]{:S(2)}) %collective-permute-start.2) | collective-permute-done | bytes 327712 | tf_op jit(solution)/shard_map/ppermute | solution.py:45
  95.7 0.7 copy-done.14
  96.5 2.4 lead.1
  98.9 8.6 %collective-permute-done.3.rest_3_ = bf16[256,640]{1,0:T(8,128)(2,1)S(1)} collective-permute-done((bf16[256,640]{1,0:T(8,128)(2,1)}, bf16[256,640]{1,0:T(8,128)(2,1)S(1)}, u32[]{:S(2)}, u32[]{:S(2)}) %collective-permute-start.3) | collective-permute-done | bytes 327712 | tf_op jit(solution)/shard_map/ppermute | solution.py:25
  107.5 0.7 copy-done.29
  108.3 13.4 %emit.1 = bf16[768,512]{1,0:T(8,128)(2,1)} custom-call(s32[2]{0:T(128)} %pad_add_fusion.info, bf16[768,256]{1,0:T(8,128)(2,1)} %queries.1, bf16[768,256]{1,0:T(8,128)(2,1)} %keys.3, bf16[768,512]{1,0:T(8,128)(2,1)} %values.3, f32[8,768]{1,0:T(8,128)} %maximum_maximum_fusion.gates, bf16[768,512]{1,0:T(8,128)(2,1)} %out_gate.1, f32[1,512]{1,0:T(1,128)} %bitcast.17, ...), custom_call_target="tpu_custom_call" | custom-call | tf_op jit(solution)/shard_map/emit/pallas_call | solution.py:262
  121.6 2.0 constant_dynamic-slice_fusion.4
  123.6 1.5 collective-permute-start.5
  126.1 5.3 %collective-permute-done.5.refs_2_ = bf16[192,512]{1,0:T(8,128)(2,1)S(1)} collective-permute-done((bf16[192,512]{1,0:T(8,128)(2,1)S(1)}, bf16[192,512]{1,0:T(8,128)(2,1)S(1)}, u32[]{:S(2)}, u32[]{:S(2)}) %collective-permute-start.5) | collective-permute-done | bytes 196640 | tf_op jit(solution)/shard_map/ppermute | solution.py:33
  131.4 3.3 collective-permute-done.6.refs_3_
  135.3 7.7 %project.1 = (f32[192,2048]{1,0:T(8,128)}, bf16[192,2048]{1,0:T(8,128)(2,1)}, bf16[192,2048]{1,0:T(8,128)(2,1)}) custom-call(s32[8]{0:T(128)} %stack.44.info, bf16[192,512]{1,0:T(8,128)(2,1)} %get-tuple-element.46.refs_0_, bf16[192,512]{1,0:T(8,128)(2,1)} %copy-done.30, bf16[192,512]{1,0:T(8,128)(2,1)} %copy-done.31, bf16[192,512]{1,0:T(8,128)(2,1)} %copy-done.32, ...), custom_call_target="tpu_custom_call" | custom-call | tf_op jit(solution)/shard_map/project/pallas_call | solution.py:314
  143.1 1.6 collective-permute-start.11
  144.8 2.8 collective-permute-start.17
  147.6 1.8 collective-permute-start.15
  149.5 25.4 %collective-permute-done.10 = bf16[192,2048]{1,0:T(8,128)(2,1)S(1)} collective-permute-done((bf16[192,2048]{1,0:T(8,128)(2,1)}, bf16[192,2048]{1,0:T(8,128)(2,1)S(1)}, u32[]{:S(2)}, u32[]{:S(2)}) %collective-permute-start.10) | collective-permute-done | bytes 786464 | tf_op jit(solution)/shard_map/ppermute | solution.py:38
  175.0 0.9 copy-done.19
  175.9 1.9 collective-permute-start.32
  177.8 1.3 constant_dynamic-update-slice_fusion.1
  179.1 1.2 constant_dynamic-update-slice_fusion.refs_1_
  180.3 17.1 %collective-permute-done.14.refs_5_.refs_3_ = bf16[256,1024]{1,0:T(8,128)(2,1)S(1)} collective-permute-done((bf16[256,1024]{1,0:T(8,128)(2,1)S(1)}, bf16[256,1024]{1,0:T(8,128)(2,1)S(1)}, u32[]{:S(2)}, u32[]{:S(2)}) %collective-permute-start.14) | collective-permute-done | bytes 524320 | tf_op jit(solution)/shard_map/ppermute | solution.py:38
  197.4 1.5 collective-permute-start.21
  199.3 8.8 %collective-permute-done.23.refs_1_ = bf16[1024,256]{1,0:T(8,128)(2,1)S(1)} collective-permute-done((bf16[1024,256]{1,0:T(8,128)(2,1)S(1)}, bf16[1024,256]{1,0:T(8,128)(2,1)S(1)}, u32[]{:S(2)}, u32[]{:S(2)}) %collective-permute-start.23) | collective-permute-done | bytes 524320 | tf_op jit(solution)/shard_map/ppermute | solution.py:38
  208.4 1.7 collective-permute-start.19
  210.1 20.9 %collective-permute-done.18.refs_9_.refs_7_ = bf16[256,1024]{1,0:T(8,128)(2,1)S(1)} collective-permute-done((bf16[256,1024]{1,0:T(8,128)(2,1)S(1)}, bf16[256,1024]{1,0:T(8,128)(2,1)S(1)}, u32[]{:S(2)}, u32[]{:S(2)}) %collective-permute-start.18) | collective-permute-done | bytes 524320 | tf_op jit(solution)/shard_map/ppermute | solution.py:33
  231.0 1.8 collective-permute-start.20
  233.4 22.6 %collective-permute-done.33.refs_1_ = bf16[1024,256]{1,0:T(8,128)(2,1)} collective-permute-done((bf16[1024,256]{1,0:T(8,128)(2,1)S(1)}, bf16[1024,256]{1,0:T(8,128)(2,1)}, u32[]{:S(2)}, u32[]{:S(2)}) %collective-permute-start.33) | collective-permute-done | bytes 524320 | tf_op jit(solution)/shard_map/ppermute | solution.py:33
  256.0 1.0 collective-permute-start.37
  257.0 1.0 collective-permute-start.38
  258.1 5.8 %shard_map.128.late = bf16[384,1024]{1,0:T(8,128)(2,1)} custom-call(bf16[192,2048]{1,0:T(8,128)(2,1)} %copy-done.18, bf16[192,2048]{1,0:T(8,128)(2,1)} %collective-permute-done.22.refs_1_, bf16[256,1024]{1,0:T(8,128)(2,1)} %copy-done, bf16[256,1024]{1,0:T(8,128)(2,1)} %copy-done.4, bf16[256,1024]{1,0:T(8,128)(2,1)} %copy-done.3, ...), custom_call_target="tpu_custom_call" | custom-call | tf_op jit(solution)/shard_map/pallas_call | solution.py:364
  263.9 10.5 %shard_map.127.early = bf16[1152,1024]{1,0:T(8,128)(2,1)} custom-call(bf16[192,2048]{1,0:T(8,128)(2,1)} %get-tuple-element.21.refs_0_, bf16[384,2048]{1,0:T(8,128)(2,1)} %copy-done.1, bf16[192,2048]{1,0:T(8,128)(2,1)} %collective-permute-done.12.refs_2_, bf16[384,2048]{1,0:T(8,128)(2,1)} %collective-permute-done.13.refs_3_, bf16[256,1024]{1,0:T(8,128)(2,1)} %copy-done, ...), custom_call_target="tpu_custom_call" | custom-call | tf_op jit(solution)/shard_map/pallas_call | solution.py:364
  274.5 6.9 %collective-permute-done.38.refs_1_ = bf16[1024,256]{1,0:T(8,128)(2,1)} collective-permute-done((bf16[1024,256]{1,0:T(8,128)(2,1)}, bf16[1024,256]{1,0:T(8,128)(2,1)}, u32[]{:S(2)}, u32[]{:S(2)}) %collective-permute-start.38) | collective-permute-done | bytes 524320 | tf_op jit(solution)/shard_map/ppermute | solution.py:25
  281.4 5.0 %shard_map.132 = (bf16[768,512]{1,0:T(8,128)(2,1)}, bf16[768,512]{1,0:T(8,128)(2,1)}) custom-call(bf16[1152,1024]{1,0:T(8,128)(2,1)} %shard_map.127.early, bf16[384,1024]{1,0:T(8,128)(2,1)} %shard_map.128.late, bf16[1024,256]{1,0:T(8,128)(2,1)} %collective-permute-done.37.refs_0_, bf16[1024,256]{1,0:T(8,128)(2,1)} %collective-permute-done.38.refs_1_), custom_call_target="tpu_custom_call" | custom-call | tf_op jit(solution)/shard_map/pallas_call | solution.py:397
  286.4 1.1 collective-permute-start.27
  287.5 1.0 collective-permute-start.28
  288.5 5.1 %shard_map.131 = (bf16[768,512]{1,0:T(8,128)(2,1)}, bf16[768,512]{1,0:T(8,128)(2,1)}) custom-call(bf16[1152,1024]{1,0:T(8,128)(2,1)} %shard_map.127.early, bf16[384,1024]{1,0:T(8,128)(2,1)} %shard_map.128.late, bf16[1024,256]{1,0:T(8,128)(2,1)} %collective-permute-done.32.refs_0_, bf16[1024,256]{1,0:T(8,128)(2,1)} %collective-permute-done.33.refs_1_), custom_call_target="tpu_custom_call" | custom-call | tf_op jit(solution)/shard_map/pallas_call | solution.py:397
  293.6 7.6 %collective-permute-done.27.refs_0_ = bf16[1024,256]{1,0:T(8,128)(2,1)S(1)} collective-permute-done((bf16[1024,256]{1,0:T(8,128)(2,1)S(1)}, bf16[1024,256]{1,0:T(8,128)(2,1)S(1)}, u32[]{:S(2)}, u32[]{:S(2)}) %collective-permute-start.27) | collective-permute-done | bytes 524320 | tf_op jit(solution)/shard_map/ppermute | solution.py:25
  301.2 10.8 %collective-permute-done.28.refs_1_ = bf16[1024,256]{1,0:T(8,128)(2,1)} collective-permute-done((bf16[1024,256]{1,0:T(8,128)(2,1)S(1)}, bf16[1024,256]{1,0:T(8,128)(2,1)}, u32[]{:S(2)}, u32[]{:S(2)}) %collective-permute-start.28) | collective-permute-done | bytes 524320 | tf_op jit(solution)/shard_map/ppermute | solution.py:25
  312.1 4.9 %shard_map.130 = (bf16[768,512]{1,0:T(8,128)(2,1)}, bf16[768,512]{1,0:T(8,128)(2,1)}) custom-call(bf16[1152,1024]{1,0:T(8,128)(2,1)} %shard_map.127.early, bf16[384,1024]{1,0:T(8,128)(2,1)} %shard_map.128.late, bf16[1024,256]{1,0:T(8,128)(2,1)} %copy-done.28, bf16[1024,256]{1,0:T(8,128)(2,1)} %collective-permute-done.28.refs_1_), custom_call_target="tpu_custom_call" | custom-call | tf_op jit(solution)/shard_map/pallas_call | solution.py:397
  317.0 5.0 %shard_map.129 = (bf16[768,512]{1,0:T(8,128)(2,1)}, bf16[768,512]{1,0:T(8,128)(2,1)}) custom-call(bf16[1152,1024]{1,0:T(8,128)(2,1)} %shard_map.127.early, bf16[384,1024]{1,0:T(8,128)(2,1)} %shard_map.128.late, bf16[1024,256]{1,0:T(8,128)(2,1)} %copy-done.10, bf16[1024,256]{1,0:T(8,128)(2,1)} %copy-done.26), custom_call_target="tpu_custom_call" | custom-call | tf_op jit(solution)/shard_map/pallas_call | solution.py:397
  322.9 0.9 copy-done.23
  324.2 1.6 collective-permute-start.35
  325.8 1.4 convert_add_fusion.2
  327.3 1.1 collective-permute-start.30
  328.7 0.8 collective-permute-start.25
  329.6 5.3 %collective-permute-done.40 = bf16[384,512]{1,0:T(8,128)(2,1)S(1)} collective-permute-done((bf16[384,512]{1,0:T(8,128)(2,1)S(1)}, bf16[384,512]{1,0:T(8,128)(2,1)S(1)}, u32[]{:S(2)}, u32[]{:S(2)}) %collective-permute-start.40) | collective-permute-done | bytes 393248 | tf_op jit(solution)/shard_map/ppermute | solution.py:38
  335.1 1.6 collective-permute-start.41
  336.8 0.7 collective-permute-start.36
  337.5 7.2 %collective-permute-done.25 = bf16[384,512]{1,0:T(8,128)(2,1)S(1)} collective-permute-done((bf16[384,512]{1,0:T(8,128)(2,1)S(1)}, bf16[384,512]{1,0:T(8,128)(2,1)S(1)}, u32[]{:S(2)}, u32[]{:S(2)}) %collective-permute-start.25) | collective-permute-done | bytes 393248 | tf_op jit(solution)/shard_map/ppermute | solution.py:33
  344.8 1.1 collective-permute-start.26
  346.1 1.6 collective-permute-start.31
  347.7 3.2 collective-permute-done.26
  351.1 1.1 collective-permute-done.31
  352.7 0.9 copy-done.21
  (145 shorter events, 8.5 us)
Async XLA Ops:
  0.0 48.8 %collective-permute-start.8 = (bf16[512,2048]{1,0:T(8,128)(2,1)}, bf16[512,2048]{1,0:T(8,128)(2,1)S(1)}, u32[]{:S(2)}, u32[]{:S(2)}) collective-permute-start(bf16[512,2048]{1,0:T(8,128)(2,1)} %refs_4_.1), channel_id=1, source_target_pairs={{0,2},{1,3},{2,0},{3,1},{4,6},{5,7},{6,4},{7,5},{8,10},{9,11},{10,... | collective-permute-start | bytes 6291464 | tf_op jit(solution)/shard_map/ppermute | solution.py:33
  3.0 131.7 %collective-permute-start.7 = (bf16[512,2048]{1,0:T(8,128)(2,1)}, bf16[512,2048]{1,0:T(8,128)(2,1)}, u32[]{:S(2)}, u32[]{:S(2)}) collective-permute-start(bf16[512,2048]{1,0:T(8,128)(2,1)} %refs_4_.1), channel_id=1, source_target_pairs={{0,1},{1,0},{2,3},{3,2},{4,5},{5,4},{6,7},{7,6},{8,9},{9,8},{10,11... | collective-permute-start | bytes 6291464 | tf_op jit(solution)/shard_map/ppermute | solution.py:25
  48.8 50.1 %copy-start.9 = (bf16[512,2048]{1,0:T(8,128)(2,1)}, bf16[512,2048]{1,0:T(8,128)(2,1)S(1)}, u32[]{:S(2)}) copy-start(bf16[512,2048]{1,0:T(8,128)(2,1)S(1)} %collective-permute-done.8.refs_6_) | copy-start | bytes 6291460
  48.8 85.9 %collective-permute-start.9 = (bf16[512,2048]{1,0:T(8,128)(2,1)S(1)}, bf16[512,2048]{1,0:T(8,128)(2,1)}, u32[]{:S(2)}, u32[]{:S(2)}) collective-permute-start(bf16[512,2048]{1,0:T(8,128)(2,1)S(1)} %collective-permute-done.8.refs_6_), channel_id=1, source_target_pairs={{0,1},{1,0},{2,3},{3,2},{4,5},{5,4},{6,7},{7,6},{8,9},{9,8},{10,11... | collective-permute-start | bytes 6291464 | tf_op jit(solution)/shard_map/ppermute | solution.py:25
  55.6 10.4 %collective-permute-start = (bf16[256,640]{1,0:T(8,128)(2,1)}, bf16[256,640]{1,0:T(8,128)(2,1)S(1)}, u32[]{:S(2)}, u32[]{:S(2)}) collective-permute-start(bf16[256,640]{1,0:T(8,128)(2,1)} %get-tuple-element.18), channel_id=1, source_target_pairs={{0,4},{4,0},{8,12},{12,8},{16,20},{20,16},{24,28},{28,24},{1,5},{5... | collective-permute-start | bytes 983048 | tf_op jit(solution)/shard_map/ppermute | solution.py:25
  69.1 11.6 %collective-permute-start.1 = (bf16[256,640]{1,0:T(8,128)(2,1)}, bf16[256,640]{1,0:T(8,128)(2,1)S(1)}, u32[]{:S(2)}, u32[]{:S(2)}) collective-permute-start(bf16[256,640]{1,0:T(8,128)(2,1)} %pair.1), channel_id=1, source_target_pairs={{8,0},{16,8},{24,16},{4,12},{12,20},{20,28},{9,1},{17,9},{25,17},{... | collective-permute-start | bytes 983048 | tf_op jit(solution)/shard_map/ppermute | solution.py:45
  70.4 25.3 %collective-permute-start.2 = (bf16[256,640]{1,0:T(8,128)(2,1)}, bf16[256,640]{1,0:T(8,128)(2,1)S(1)}, u32[]{:S(2)}, u32[]{:S(2)}) collective-permute-start(bf16[256,640]{1,0:T(8,128)(2,1)} %pair.1), channel_id=1, source_target_pairs={{16,0},{24,8},{4,20},{12,28},{17,1},{25,9},{5,21},{13,29},{18,2},{... | collective-permute-start | bytes 983048 | tf_op jit(solution)/shard_map/ppermute | solution.py:45
  80.7 15.1 %copy-start.13 = (bf16[256,640]{1,0:T(8,128)(2,1)}, bf16[256,640]{1,0:T(8,128)(2,1)S(1)}, u32[]{:S(2)}) copy-start(bf16[256,640]{1,0:T(8,128)(2,1)S(1)} %collective-permute-done.1.refs_0_.rest_1_) | copy-start | bytes 983044
  98.9 8.6 %collective-permute-start.3 = (bf16[256,640]{1,0:T(8,128)(2,1)}, bf16[256,640]{1,0:T(8,128)(2,1)S(1)}, u32[]{:S(2)}, u32[]{:S(2)}) collective-permute-start(bf16[256,640]{1,0:T(8,128)(2,1)} %lead.1), channel_id=1, source_target_pairs={{0,4},{4,0},{8,12},{12,8},{16,20},{20,16},{24,28},{28,24},{1,5},{5... | collective-permute-start | bytes 983048 | tf_op jit(solution)/shard_map/ppermute | solution.py:25
  123.6 2.5 collective-permute-start.4
  123.6 7.8 %collective-permute-start.5 = (bf16[192,512]{1,0:T(8,128)(2,1)S(1)}, bf16[192,512]{1,0:T(8,128)(2,1)S(1)}, u32[]{:S(2)}, u32[]{:S(2)}) collective-permute-start(bf16[192,512]{1,0:T(8,128)(2,1)S(1)} %get-tuple-element.44), channel_id=1, source_target_pairs={{0,2},{1,3},{2,0},{3,1},{4,6},{5,7},{6,4},{7,5},{8,10},{9,11},{10,... | collective-permute-start | bytes 589832 | tf_op jit(solution)/shard_map/ppermute | solution.py:33
  125.1 9.5 %collective-permute-start.6 = (bf16[192,512]{1,0:T(8,128)(2,1)S(1)}, bf16[192,512]{1,0:T(8,128)(2,1)S(1)}, u32[]{:S(2)}, u32[]{:S(2)}) collective-permute-start(bf16[192,512]{1,0:T(8,128)(2,1)S(1)} %get-tuple-element.43), channel_id=1, source_target_pairs={{0,3},{1,2},{2,1},{3,0},{4,7},{5,6},{6,5},{7,4},{8,11},{9,10},{10,... | collective-permute-start | bytes 589832 | tf_op jit(solution)/shard_map/ppermute | solution.py:33
  126.1 8.6 %copy-start.30 = (bf16[192,512]{1,0:T(8,128)(2,1)}, bf16[192,512]{1,0:T(8,128)(2,1)S(1)}, u32[]{:S(2)}) copy-start(bf16[192,512]{1,0:T(8,128)(2,1)S(1)} %collective-permute-done.4.refs_1_) | copy-start | bytes 589828
  131.4 3.3 copy-start.31
  135.3 9.4 %copy-start.16 = (bf16[256,2048]{1,0:T(8,128)(2,1)S(1)}, bf16[256,2048]{1,0:T(8,128)(2,1)}, u32[]{:S(2)}) copy-start(bf16[256,2048]{1,0:T(8,128)(2,1)} %param.24) | copy-start | bytes 3145732
  143.1 6.4 %copy-start.17 = (bf16[2048,256]{1,0:T(8,128)(2,1)S(1)}, bf16[2048,256]{1,0:T(8,128)(2,1)}, u32[]{:S(2)}) copy-start(bf16[2048,256]{1,0:T(8,128)(2,1)} %param.25) | copy-start | bytes 3145732
  143.1 31.9 %collective-permute-start.10 = (bf16[192,2048]{1,0:T(8,128)(2,1)}, bf16[192,2048]{1,0:T(8,128)(2,1)S(1)}, u32[]{:S(2)}, u32[]{:S(2)}) collective-permute-start(bf16[192,2048]{1,0:T(8,128)(2,1)} %get-tuple-element.22), channel_id=1, source_target_pairs={{0,8},{4,12},{8,0},{12,4},{16,24},{20,28},{24,16},{28,20},{1,9},{5... | collective-permute-start | bytes 2359304 | tf_op jit(solution)/shard_map/ppermute | solution.py:38
  143.1 31.9 %collective-permute-start.11 = (bf16[192,2048]{1,0:T(8,128)(2,1)}, bf16[192,2048]{1,0:T(8,128)(2,1)}, u32[]{:S(2)}, u32[]{:S(2)}) collective-permute-start(bf16[192,2048]{1,0:T(8,128)(2,1)} %get-tuple-element.21.refs_0_), channel_id=1, source_target_pairs={{0,2},{1,3},{2,0},{3,1},{4,6},{5,7},{6,4},{7,5},{8,10},{9,11},{10,... | collective-permute-start | bytes 2359304 | tf_op jit(solution)/shard_map/ppermute | solution.py:33
  144.8 34.3 %copy-start = (bf16[256,1024]{1,0:T(8,128)(2,1)}, bf16[256,1024]{1,0:T(8,128)(2,1)S(1)}, u32[]{:S(2)}) copy-start(bf16[256,1024]{1,0:T(8,128)(2,1)S(1)} %get-tuple-element.38.refs_4_.refs_2_) | copy-start | bytes 1572868
  144.8 54.2 %collective-permute-start.17 = (bf16[256,1024]{1,0:T(8,128)(2,1)S(1)}, bf16[256,1024]{1,0:T(8,128)(2,1)S(1)}, u32[]{:S(2)}, u32[]{:S(2)}) collective-permute-start(bf16[256,1024]{1,0:T(8,128)(2,1)S(1)} %get-tuple-element.38.refs_4_.refs_2_), channel_id=1, source_target_pairs={{0,16},{4,20},{8,24},{12,28},{16,0},{20,4},{24,8},{28,12},{1,17},{... | collective-permute-start | bytes 1572872 | tf_op jit(solution)/shard_map/ppermute | solution.py:33
  147.6 51.7 %collective-permute-start.15 = (bf16[256,1024]{1,0:T(8,128)(2,1)S(1)}, bf16[256,1024]{1,0:T(8,128)(2,1)S(1)}, u32[]{:S(2)}, u32[]{:S(2)}) collective-permute-start(bf16[256,1024]{1,0:T(8,128)(2,1)S(1)} %get-tuple-element.38.refs_4_.refs_2_), channel_id=1, source_target_pairs={{0,4},{4,0},{8,12},{12,8},{16,20},{20,16},{24,28},{28,24},{1,5},{5... | collective-permute-start | bytes 1572872 | tf_op jit(solution)/shard_map/ppermute | solution.py:25
  149.4 48.1 %collective-permute-start.14 = (bf16[256,1024]{1,0:T(8,128)(2,1)S(1)}, bf16[256,1024]{1,0:T(8,128)(2,1)S(1)}, u32[]{:S(2)}, u32[]{:S(2)}) collective-permute-start(bf16[256,1024]{1,0:T(8,128)(2,1)S(1)} %get-tuple-element.37), channel_id=1, source_target_pairs={{0,8},{4,12},{8,0},{12,4},{16,24},{20,28},{24,16},{28,20},{1,9},{5... | collective-permute-start | bytes 1572872 | tf_op jit(solution)/shard_map/ppermute | solution.py:38
  149.5 30.7 %copy-start.10 = (bf16[1024,256]{1,0:T(8,128)(2,1)}, bf16[1024,256]{1,0:T(8,128)(2,1)S(1)}, u32[]{:S(2)}) copy-start(bf16[1024,256]{1,0:T(8,128)(2,1)S(1)} %get-tuple-element.36.refs_0_) | copy-start | bytes 1572868
  175.0 33.1 %collective-permute-start.23 = (bf16[1024,256]{1,0:T(8,128)(2,1)S(1)}, bf16[1024,256]{1,0:T(8,128)(2,1)S(1)}, u32[]{:S(2)}, u32[]{:S(2)}) collective-permute-start(bf16[1024,256]{1,0:T(8,128)(2,1)S(1)} %get-tuple-element.35), channel_id=1, source_target_pairs={{0,8},{4,12},{8,0},{12,4},{16,24},{20,28},{24,16},{28,20},{1,9},{5... | collective-permute-start | bytes 1572872 | tf_op jit(solution)/shard_map/ppermute | solution.py:38
  175.9 32.5 %collective-permute-start.32 = (bf16[1024,256]{1,0:T(8,128)(2,1)S(1)}, bf16[1024,256]{1,0:T(8,128)(2,1)}, u32[]{:S(2)}, u32[]{:S(2)}) collective-permute-start(bf16[1024,256]{1,0:T(8,128)(2,1)S(1)} %get-tuple-element.36.refs_0_), channel_id=1, source_target_pairs={{0,16},{4,20},{8,24},{12,28},{16,0},{20,4},{24,8},{28,12},{1,17},{... | collective-permute-start | bytes 1572872 | tf_op jit(solution)/shard_map/ppermute | solution.py:33
  177.8 19.6 %copy-start.20 = (bf16[192,2048]{1,0:T(8,128)(2,1)S(1)}, bf16[192,2048]{1,0:T(8,128)(2,1)}, u32[]{:S(2)}) copy-start(bf16[192,2048]{1,0:T(8,128)(2,1)} %copy-done.19) | copy-start | bytes 2359300
  180.3 83.6 %copy-start.1 = (bf16[384,2048]{1,0:T(8,128)(2,1)}, bf16[384,2048]{1,0:T(8,128)(2,1)S(1)}, u32[]{:S(2)}) copy-start(bf16[384,2048]{1,0:T(8,128)(2,1)S(1)} %constant_dynamic-update-slice_fusion.refs_1_) | copy-start | bytes 4718596
  197.4 60.7 %copy-start.4 = (bf16[256,1024]{1,0:T(8,128)(2,1)}, bf16[256,1024]{1,0:T(8,128)(2,1)S(1)}, u32[]{:S(2)}) copy-start(bf16[256,1024]{1,0:T(8,128)(2,1)S(1)} %collective-permute-done.14.refs_5_.refs_3_) | copy-start | bytes 1572868
  197.4 35.4 %collective-permute-start.21 = (bf16[192,2048]{1,0:T(8,128)(2,1)S(1)}, bf16[192,2048]{1,0:T(8,128)(2,1)S(1)}, u32[]{:S(2)}, u32[]{:S(2)}) collective-permute-start(bf16[192,2048]{1,0:T(8,128)(2,1)S(1)} %copy-done.20), channel_id=1, source_target_pairs={{0,2},{1,3},{2,0},{3,1},{4,6},{5,7},{6,4},{7,5},{8,10},{9,11},{10,... | collective-permute-start | bytes 2359304 | tf_op jit(solution)/shard_map/ppermute | solution.py:33
  199.0 59.2 %copy-start.2 = (bf16[256,1024]{1,0:T(8,128)(2,1)}, bf16[256,1024]{1,0:T(8,128)(2,1)S(1)}, u32[]{:S(2)}) copy-start(bf16[256,1024]{1,0:T(8,128)(2,1)S(1)} %collective-permute-done.17.refs_8_.refs_6_) | copy-start | bytes 1572868
  199.0 32.0 %collective-permute-start.18 = (bf16[256,1024]{1,0:T(8,128)(2,1)S(1)}, bf16[256,1024]{1,0:T(8,128)(2,1)S(1)}, u32[]{:S(2)}, u32[]{:S(2)}) collective-permute-start(bf16[256,1024]{1,0:T(8,128)(2,1)S(1)} %collective-permute-done.14.refs_5_.refs_3_), channel_id=1, source_target_pairs={{0,16},{4,20},{8,24},{12,28},{16,0},{20,4},{24,8},{28,12},{1,17},{... | collective-permute-start | bytes 1572872 | tf_op jit(solution)/shard_map/ppermute | solution.py:33
  199.3 58.8 %copy-start.3 = (bf16[256,1024]{1,0:T(8,128)(2,1)}, bf16[256,1024]{1,0:T(8,128)(2,1)S(1)}, u32[]{:S(2)}) copy-start(bf16[256,1024]{1,0:T(8,128)(2,1)S(1)} %collective-permute-done.15.refs_6_.refs_4_) | copy-start | bytes 1572868
  199.3 64.6 %collective-permute-start.13 = (bf16[384,2048]{1,0:T(8,128)(2,1)S(1)}, bf16[384,2048]{1,0:T(8,128)(2,1)}, u32[]{:S(2)}, u32[]{:S(2)}) collective-permute-start(bf16[384,2048]{1,0:T(8,128)(2,1)S(1)} %constant_dynamic-update-slice_fusion.refs_1_), channel_id=1, source_target_pairs={{0,1},{1,0},{2,3},{3,2},{4,5},{5,4},{6,7},{7,6},{8,9},{9,8},{10,11... | collective-permute-start | bytes 4718600 | tf_op jit(solution)/shard_map/ppermute | solution.py:25
  208.1 50.0 %copy-start.26 = (bf16[1024,256]{1,0:T(8,128)(2,1)}, bf16[1024,256]{1,0:T(8,128)(2,1)S(1)}, u32[]{:S(2)}) copy-start(bf16[1024,256]{1,0:T(8,128)(2,1)S(1)} %collective-permute-done.23.refs_1_) | copy-start | bytes 1572868
  208.1 22.9 %collective-permute-start.16 = (bf16[256,1024]{1,0:T(8,128)(2,1)S(1)}, bf16[256,1024]{1,0:T(8,128)(2,1)S(1)}, u32[]{:S(2)}, u32[]{:S(2)}) collective-permute-start(bf16[256,1024]{1,0:T(8,128)(2,1)S(1)} %collective-permute-done.14.refs_5_.refs_3_), channel_id=1, source_target_pairs={{0,4},{4,0},{8,12},{12,8},{16,20},{20,16},{24,28},{28,24},{1,5},{5... | collective-permute-start | bytes 1572872 | tf_op jit(solution)/shard_map/ppermute | solution.py:25
  208.4 24.4 %collective-permute-start.19 = (bf16[256,1024]{1,0:T(8,128)(2,1)S(1)}, bf16[256,1024]{1,0:T(8,128)(2,1)S(1)}, u32[]{:S(2)}, u32[]{:S(2)}) collective-permute-start(bf16[256,1024]{1,0:T(8,128)(2,1)S(1)} %collective-permute-done.17.refs_8_.refs_6_), channel_id=1, source_target_pairs={{0,4},{4,0},{8,12},{12,8},{16,20},{20,16},{24,28},{28,24},{1,5},{5... | collective-permute-start | bytes 1572872 | tf_op jit(solution)/shard_map/ppermute | solution.py:25
  231.0 25.0 %collective-permute-start.33 = (bf16[1024,256]{1,0:T(8,128)(2,1)S(1)}, bf16[1024,256]{1,0:T(8,128)(2,1)}, u32[]{:S(2)}, u32[]{:S(2)}) collective-permute-start(bf16[1024,256]{1,0:T(8,128)(2,1)S(1)} %collective-permute-done.23.refs_1_), channel_id=1, source_target_pairs={{0,16},{4,20},{8,24},{12,28},{16,0},{20,4},{24,8},{28,12},{1,17},{... | collective-permute-start | bytes 1572872 | tf_op jit(solution)/shard_map/ppermute | solution.py:33
  231.0 26.0 %copy-start.6 = (bf16[256,1024]{1,0:T(8,128)(2,1)}, bf16[256,1024]{1,0:T(8,128)(2,1)S(1)}, u32[]{:S(2)}) copy-start(bf16[256,1024]{1,0:T(8,128)(2,1)S(1)} %collective-permute-done.16.refs_7_.refs_5_) | copy-start | bytes 1572868
  231.0 26.0 %collective-permute-start.20 = (bf16[256,1024]{1,0:T(8,128)(2,1)S(1)}, bf16[256,1024]{1,0:T(8,128)(2,1)S(1)}, u32[]{:S(2)}, u32[]{:S(2)}) collective-permute-start(bf16[256,1024]{1,0:T(8,128)(2,1)S(1)} %collective-permute-done.18.refs_9_.refs_7_), channel_id=1, source_target_pairs={{0,4},{4,0},{8,12},{12,8},{16,20},{20,16},{24,28},{28,24},{1,5},{5... | collective-permute-start | bytes 1572872 | tf_op jit(solution)/shard_map/ppermute | solution.py:25
  232.8 25.2 %copy-start.18 = (bf16[192,2048]{1,0:T(8,128)(2,1)}, bf16[192,2048]{1,0:T(8,128)(2,1)S(1)}, u32[]{:S(2)}) copy-start(bf16[192,2048]{1,0:T(8,128)(2,1)S(1)} %collective-permute-done.21.refs_0_) | copy-start | bytes 2359300
  232.8 25.2 %collective-permute-start.22 = (bf16[192,2048]{1,0:T(8,128)(2,1)S(1)}, bf16[192,2048]{1,0:T(8,128)(2,1)}, u32[]{:S(2)}, u32[]{:S(2)}) collective-permute-start(bf16[192,2048]{1,0:T(8,128)(2,1)S(1)} %collective-permute-done.21.refs_0_), channel_id=1, source_target_pairs={{0,1},{1,0},{2,3},{3,2},{4,5},{5,4},{6,7},{7,6},{8,9},{9,8},{10,11... | collective-permute-start | bytes 2359304 | tf_op jit(solution)/shard_map/ppermute | solution.py:25
  232.9 25.2 %copy-start.7 = (bf16[256,1024]{1,0:T(8,128)(2,1)}, bf16[256,1024]{1,0:T(8,128)(2,1)S(1)}, u32[]{:S(2)}) copy-start(bf16[256,1024]{1,0:T(8,128)(2,1)S(1)} %collective-permute-done.19.refs_10_.refs_8_) | copy-start | bytes 1572868
  232.9 31.0 %collective-permute-start.12 = (bf16[192,2048]{1,0:T(8,128)(2,1)}, bf16[192,2048]{1,0:T(8,128)(2,1)}, u32[]{:S(2)}, u32[]{:S(2)}) collective-permute-start(bf16[192,2048]{1,0:T(8,128)(2,1)} %get-tuple-element.21.refs_0_), channel_id=1, source_target_pairs={{0,1},{1,0},{2,3},{3,2},{4,5},{5,4},{6,7},{7,6},{8,9},{9,8},{10,11... | collective-permute-start | bytes 2359304 | tf_op jit(solution)/shard_map/ppermute | solution.py:25
  256.0 18.5 %collective-permute-start.37 = (bf16[1024,256]{1,0:T(8,128)(2,1)}, bf16[1024,256]{1,0:T(8,128)(2,1)}, u32[]{:S(2)}, u32[]{:S(2)}) collective-permute-start(bf16[1024,256]{1,0:T(8,128)(2,1)} %collective-permute-done.32.refs_0_), channel_id=1, source_target_pairs={{0,4},{4,0},{8,12},{12,8},{16,20},{20,16},{24,28},{28,24},{1,5},{5... | collective-permute-start | bytes 1572872 | tf_op jit(solution)/shard_map/ppermute | solution.py:25
  257.0 24.4 %collective-permute-start.38 = (bf16[1024,256]{1,0:T(8,128)(2,1)}, bf16[1024,256]{1,0:T(8,128)(2,1)}, u32[]{:S(2)}, u32[]{:S(2)}) collective-permute-start(bf16[1024,256]{1,0:T(8,128)(2,1)} %collective-permute-done.33.refs_1_), channel_id=1, source_target_pairs={{0,4},{4,0},{8,12},{12,8},{16,20},{20,16},{24,28},{28,24},{1,5},{5... | collective-permute-start | bytes 1572872 | tf_op jit(solution)/shard_map/ppermute | solution.py:25
  274.4 11.9 %copy-start.11 = (bf16[1024,256]{1,0:T(8,128)(2,1)S(1)}, bf16[1024,256]{1,0:T(8,128)(2,1)}, u32[]{:S(2)}) copy-start(bf16[1024,256]{1,0:T(8,128)(2,1)} %copy-done.10) | copy-start | bytes 1572868
  274.4 13.0 %copy-start.27 = (bf16[1024,256]{1,0:T(8,128)(2,1)S(1)}, bf16[1024,256]{1,0:T(8,128)(2,1)}, u32[]{:S(2)}) copy-start(bf16[1024,256]{1,0:T(8,128)(2,1)} %copy-done.26) | copy-start | bytes 1572868
  286.4 36.1 %collective-permute-start.39 = (bf16[768,512]{1,0:T(8,128)(2,1)}, bf16[768,512]{1,0:T(8,128)(2,1)S(1)}, u32[]{:S(2)}, u32[]{:S(2)}) collective-permute-start(bf16[768,512]{1,0:T(8,128)(2,1)} %get-tuple-element.30), channel_id=1, source_target_pairs={{0,1},{1,0},{2,3},{3,2},{4,5},{5,4},{6,7},{7,6},{8,9},{9,8},{10,11... | collective-permute-start | bytes 2359304 | tf_op jit(solution)/shard_map/ppermute | solution.py:25
  286.4 14.9 %collective-permute-start.27 = (bf16[1024,256]{1,0:T(8,128)(2,1)S(1)}, bf16[1024,256]{1,0:T(8,128)(2,1)S(1)}, u32[]{:S(2)}, u32[]{:S(2)}) collective-permute-start(bf16[1024,256]{1,0:T(8,128)(2,1)S(1)} %copy-done.11), channel_id=1, source_target_pairs={{0,4},{4,0},{8,12},{12,8},{16,20},{20,16},{24,28},{28,24},{1,5},{5... | collective-permute-start | bytes 1572872 | tf_op jit(solution)/shard_map/ppermute | solution.py:25
  287.5 24.6 %collective-permute-start.28 = (bf16[1024,256]{1,0:T(8,128)(2,1)S(1)}, bf16[1024,256]{1,0:T(8,128)(2,1)}, u32[]{:S(2)}, u32[]{:S(2)}) collective-permute-start(bf16[1024,256]{1,0:T(8,128)(2,1)S(1)} %copy-done.27), channel_id=1, source_target_pairs={{0,4},{4,0},{8,12},{12,8},{16,20},{20,16},{24,28},{28,24},{1,5},{5... | collective-permute-start | bytes 1572872 | tf_op jit(solution)/shard_map/ppermute | solution.py:25
  293.6 29.3 %collective-permute-start.34 = (bf16[768,512]{1,0:T(8,128)(2,1)}, bf16[768,512]{1,0:T(8,128)(2,1)S(1)}, u32[]{:S(2)}, u32[]{:S(2)}) collective-permute-start(bf16[768,512]{1,0:T(8,128)(2,1)} %get-tuple-element.28), channel_id=1, source_target_pairs={{0,1},{1,0},{2,3},{3,2},{4,5},{5,4},{6,7},{7,6},{8,9},{9,8},{10,11... | collective-permute-start | bytes 2359304 | tf_op jit(solution)/shard_map/ppermute | solution.py:25
  301.2 10.8 %copy-start.28 = (bf16[1024,256]{1,0:T(8,128)(2,1)}, bf16[1024,256]{1,0:T(8,128)(2,1)S(1)}, u32[]{:S(2)}) copy-start(bf16[1024,256]{1,0:T(8,128)(2,1)S(1)} %collective-permute-done.27.refs_0_) | copy-start | bytes 1572868
  316.9 5.5 %copy-start.24 = (bf16[768,512]{1,0:T(8,128)(2,1)S(1)}, bf16[768,512]{1,0:T(8,128)(2,1)}, u32[]{:S(2)}) copy-start(bf16[768,512]{1,0:T(8,128)(2,1)} %get-tuple-element.29) | copy-start | bytes 2359300
  316.9 8.8 %collective-permute-start.29 = (bf16[768,512]{1,0:T(8,128)(2,1)}, bf16[768,512]{1,0:T(8,128)(2,1)}, u32[]{:S(2)}, u32[]{:S(2)}) collective-permute-start(bf16[768,512]{1,0:T(8,128)(2,1)} %get-tuple-element.26), channel_id=1, source_target_pairs={{0,1},{1,0},{2,3},{3,2},{4,5},{5,4},{6,7},{7,6},{8,9},{9,8},{10,11... | collective-permute-start | bytes 2359304 | tf_op jit(solution)/shard_map/ppermute | solution.py:25
  322.0 6.5 %collective-permute-start.24 = (bf16[768,512]{1,0:T(8,128)(2,1)}, bf16[768,512]{1,0:T(8,128)(2,1)S(1)}, u32[]{:S(2)}, u32[]{:S(2)}) collective-permute-start(bf16[768,512]{1,0:T(8,128)(2,1)} %get-tuple-element.24), channel_id=1, source_target_pairs={{0,1},{1,0},{2,3},{3,2},{4,5},{5,4},{6,7},{7,6},{8,9},{9,8},{10,11... | collective-permute-start | bytes 2359304 | tf_op jit(solution)/shard_map/ppermute | solution.py:25
  322.9 12.1 %collective-permute-start.40 = (bf16[384,512]{1,0:T(8,128)(2,1)S(1)}, bf16[384,512]{1,0:T(8,128)(2,1)S(1)}, u32[]{:S(2)}, u32[]{:S(2)}) collective-permute-start(bf16[384,512]{1,0:T(8,128)(2,1)S(1)} %fusion.2), channel_id=1, source_target_pairs={{0,8},{4,12},{8,0},{12,4},{16,24},{20,28},{24,16},{28,20},{1,9},{5... | collective-permute-start | bytes 1179656 | tf_op jit(solution)/shard_map/ppermute | solution.py:38
  324.2 12.5 %collective-permute-start.35 = (bf16[384,512]{1,0:T(8,128)(2,1)S(1)}, bf16[384,512]{1,0:T(8,128)(2,1)S(1)}, u32[]{:S(2)}, u32[]{:S(2)}) collective-permute-start(bf16[384,512]{1,0:T(8,128)(2,1)S(1)} %concatenate.46), channel_id=1, source_target_pairs={{0,2},{1,3},{2,0},{3,1},{4,6},{5,7},{6,4},{7,5},{8,10},{9,11},{10,... | collective-permute-start | bytes 1179656 | tf_op jit(solution)/shard_map/ppermute | solution.py:33
  327.3 18.6 %collective-permute-start.30 = (bf16[384,512]{1,0:T(8,128)(2,1)S(1)}, bf16[384,512]{1,0:T(8,128)(2,1)S(1)}, u32[]{:S(2)}, u32[]{:S(2)}) collective-permute-start(bf16[384,512]{1,0:T(8,128)(2,1)S(1)} %fusion.7), channel_id=1, source_target_pairs={{0,8},{4,12},{8,0},{12,4},{16,24},{20,28},{24,16},{28,20},{1,9},{5... | collective-permute-start | bytes 1179656 | tf_op jit(solution)/shard_map/ppermute | solution.py:38
  328.7 15.9 %collective-permute-start.25 = (bf16[384,512]{1,0:T(8,128)(2,1)S(1)}, bf16[384,512]{1,0:T(8,128)(2,1)S(1)}, u32[]{:S(2)}, u32[]{:S(2)}) collective-permute-start(bf16[384,512]{1,0:T(8,128)(2,1)S(1)} %concatenate.47), channel_id=1, source_target_pairs={{0,2},{1,3},{2,0},{3,1},{4,6},{5,7},{6,4},{7,5},{8,10},{9,11},{10,... | collective-permute-start | bytes 1179656 | tf_op jit(solution)/shard_map/ppermute | solution.py:33
  335.1 17.5 %collective-permute-start.41 = (bf16[192,512]{1,0:T(8,128)(2,1)S(1)}, bf16[192,512]{1,0:T(8,128)(2,1)S(1)}, u32[]{:S(2)}, u32[]{:S(2)}) collective-permute-start(bf16[192,512]{1,0:T(8,128)(2,1)S(1)} %fusion), channel_id=1, source_target_pairs={{0,2},{1,3},{2,0},{3,1},{4,6},{5,7},{6,4},{7,5},{8,10},{9,11},{10,... | collective-permute-start | bytes 589832 | tf_op jit(solution)/shard_map/ppermute | solution.py:33
  336.8 15.6 %collective-permute-start.36 = (bf16[192,512]{1,0:T(8,128)(2,1)S(1)}, bf16[192,512]{1,0:T(8,128)(2,1)S(1)}, u32[]{:S(2)}, u32[]{:S(2)}) collective-permute-start(bf16[192,512]{1,0:T(8,128)(2,1)S(1)} %pad_maximum_fusion.3), channel_id=1, source_target_pairs={{0,8},{4,12},{8,0},{12,4},{16,24},{20,28},{24,16},{28,20},{1,9},{5... | collective-permute-start | bytes 589832 | tf_op jit(solution)/shard_map/ppermute | solution.py:38
  344.8 6.1 %collective-permute-start.26 = (bf16[192,512]{1,0:T(8,128)(2,1)S(1)}, bf16[192,512]{1,0:T(8,128)(2,1)S(1)}, u32[]{:S(2)}, u32[]{:S(2)}) collective-permute-start(bf16[192,512]{1,0:T(8,128)(2,1)S(1)} %pad_maximum_fusion.2), channel_id=1, source_target_pairs={{0,8},{4,12},{8,0},{12,4},{16,24},{20,28},{24,16},{28,20},{1,9},{5... | collective-permute-start | bytes 589832 | tf_op jit(solution)/shard_map/ppermute | solution.py:38
  346.0 5.0 %copy-start.12 = (f32[192,2048]{1,0:T(8,128)S(1)}, f32[192,2048]{1,0:T(8,128)}, u32[]{:S(2)}) copy-start(f32[192,2048]{1,0:T(8,128)} %get-tuple-element.20) | copy-start | bytes 4718596
  346.1 6.1 %collective-permute-start.31 = (bf16[192,512]{1,0:T(8,128)(2,1)S(1)}, bf16[192,512]{1,0:T(8,128)(2,1)S(1)}, u32[]{:S(2)}, u32[]{:S(2)}) collective-permute-start(bf16[192,512]{1,0:T(8,128)(2,1)S(1)} %fusion.5), channel_id=1, source_target_pairs={{0,2},{1,3},{2,0},{3,1},{4,6},{5,7},{6,4},{7,5},{8,10},{9,11},{10,... | collective-permute-start | bytes 589832 | tf_op jit(solution)/shard_map/ppermute | solution.py:33
  (11 other events, 11.9 us)
